TPU v7x, 32 devices: a whole 2x2x4 slice. The times are simulated.
32 devices in a mesh: sp: 8 (over z, y), dp: 4 (over x, core).
Axes of the slice: x: 2, y: 2, z: 4, core: 2. Of those that a mesh axis runs over, the one named last changes fastest.
Arguments:
- out_cotangent: bfloat16 [4, 2048, 2048], P('dp', 'sp'), may hold values from -6 to 6
- value_pre: bfloat16 [4, 2048, 2048], P('dp', 'sp'), may hold values from -8 to 8
- gate_pre: bfloat16 [4, 2048, 2048], P('dp', 'sp'), may hold values from -8 to 8
- out_weight: bfloat16 [2048, 2048], P('dp'), may hold values from -0.125 to 0.125
- conv_kernel: bfloat16 [31, 2048], P(None, 'sp'), may hold values from -6 to 6
- norm_gain: bfloat16 [2048], P('sp'), may hold values from 0.099609375 to 1.8984375
Outputs:
- grad_value: bfloat16 [4, 2048, 2048], P('dp', 'sp')
- grad_gate: bfloat16 [4, 2048, 2048], P('dp', 'sp')
- grad_out_weight: float32 [2048, 2048], P(('sp', 'dp'))
- grad_kernel: float32 [31, 2048], P(None, 'sp')
- grad_gain: float32 [2048], P('sp')
All inputs are finite; a program needn't handle non-finite values.
Results may differ from a plain program's by a relative error of at most 0.011.
Values may be sent and summed in bfloat16 or wider, within the bound.
A program may use at most 128 MiB of HBM per device.

v0:
```python
import functools

import jax
import jax.numpy as jnp
from jax import lax
from jax.experimental import pallas as pl
from jax.experimental.pallas import tpu as pltpu
from jax.sharding import PartitionSpec as P

epsilon = 1e-05
LANES = 128
HALVES = 2
f32 = jnp.float32
bf16 = jnp.bfloat16


def block_kernel(
    S, N, T, C, K, HB, ids,
    cot, val, gate, w, taps,
    gv, gg, gw, kout, gout,
    cot_all, ext, cen, gc, gext, kall, act, act_all, ga_send, ga, wpart, rbuf,
    kg, krecv, ksum, k2recv, send_sem, recv_sem,
):
    s = lax.axis_index("sp")
    d = lax.axis_index("dp")
    chunks = C // LANES
    cps = chunks // S
    cpd = chunks // N
    block = C // (S * N)
    RB = min(T, 128)
    total = S * N
    me = s * N + d
    partner = d + 1 - 2 * lax.rem(d, 2)
    factor = float(S * N * T) ** (-0.5)
    hrows = T // HALVES
    waits = []

    def copy(src, dst, i, to_s, to_d):
        return pltpu.make_async_remote_copy(
            src_ref=src, dst_ref=dst, send_sem=send_sem.at[i], recv_sem=recv_sem.at[i],
            device_id={"sp": to_s, "dp": to_d}, device_id_type=pl.DeviceIdType.MESH,
        )

    def send(src, dst, i, to_s, to_d):
        c = copy(src, dst, i, to_s, to_d)
        c.start()
        waits.append(c)

    def arrived(dst, i):
        copy(dst, dst, i, s, partner).wait_recv()

    barrier = pltpu.get_barrier_semaphore()

    def greet(j, _):
        other = lax.rem(me + j, total)
        pl.semaphore_signal(
            barrier, inc=1, device_id={"sp": other // N, "dp": lax.rem(other, N)},
            device_id_type=pl.DeviceIdType.MESH,
        )
        return _

    lax.fori_loop(1, total, greet, 0)
    def gate_chunk(cb, _):
        cols = pl.ds(pl.multiple_of(cb * LANES, LANES), LANES)
        sig = jax.nn.sigmoid(gate[:, cols].astype(f32))
        ext[cb, pl.ds(HB, T), :] = (val[:, cols].astype(f32) * sig).astype(bf16).astype(f32)
        return _

    lax.fori_loop(0, chunks, gate_chunk, 0)
    pl.semaphore_wait(barrier, total - 1)

    for j in range(1, S):
        send(taps, kall.at[pl.ds(s * cps, cps)], ids["taps"] + j, lax.rem(s + j, S), d)
    following = lax.rem(s + 1, S)
    preceding = lax.rem(s + S - 1, S)
    send(ext.at[:, pl.ds(T, HB), :], ext.at[:, pl.ds(0, HB), :], ids["front"], following, d)
    for j in range(1, N // 2):
        for h in range(HALVES):
            rows = pl.ds(h * hrows, hrows)
            send(cot.at[rows], cot_all.at[d, rows], ids["mirror"] + j * HALVES + h, s, lax.rem(d + 2 * j, N))
    send(cot, cot_all.at[d], ids["partner"], s, partner)
    kall[pl.ds(s * cps, cps)] = taps[...]
    cot_all[d] = cot[...]
    for j in range(1, S):
        arrived(kall.at[pl.ds(lax.rem(s + S - j, S) * cps, cps)], ids["taps"] + j)
    arrived(ext.at[:, pl.ds(0, HB), :], ids["front"])

    @pl.when(s == 0)
    def _():
        ext[:, pl.ds(0, HB), :] = jnp.zeros((chunks, HB, LANES), f32)

    def conv_chunk(cb, sums):
        tf = kall[cb].astype(f32)
        parts = []
        for rb in range(T // RB):
            acc = jnp.zeros((RB, LANES), f32)
            for k in range(K):
                acc = acc + tf[k : k + 1] * ext[cb, pl.ds(HB - k + rb * RB, RB), :]
            cen[cb, pl.ds(rb * RB, RB), :] = acc
            parts.append(jnp.sum(acc, axis=1, keepdims=True))
        return sums + jnp.concatenate(parts, axis=0)

    column = jnp.zeros((T, 1), f32)
    mean = lax.fori_loop(0, chunks, conv_chunk, column) / C

    def square_chunk(cb, sums):
        dev = cen[cb] - mean
        return sums + dev * dev

    squares = lax.fori_loop(0, chunks, square_chunk, jnp.zeros((T, LANES), f32))
    inv = lax.rsqrt(jnp.sum(squares, axis=1, keepdims=True) / C + epsilon)

    def relay():
        for j in range(1, N // 2):
            origin = lax.rem(d + N - 2 * j, N)
            for h in range(HALVES):
                piece = cot_all.at[origin, pl.ds(h * hrows, hrows)]
                arrived(piece, ids["mirror"] + j * HALVES + h)
                send(piece, piece, ids["relay"] + j * HALVES + h, s, partner)

    def act_chunk(cb, _):
        centred = (cen[cb] - mean) * inv
        cen[cb] = centred
        normed = centred * kall[cb].astype(f32)[K : K + 1]
        act[cb] = (normed * jax.nn.sigmoid(normed)).astype(bf16)
        return _

    lax.fori_loop(0, chunks, act_chunk, 0)
    for j in range(1, N):
        to = lax.rem(d + j, N)
        send(act.at[pl.ds(to * cpd, cpd)], act_all.at[d], ids["act"] + j, s, to)
    act_all[d] = act[pl.ds(d * cpd, cpd)]

    def project(source, slot):
        def pair(m, _):
            rows = pl.ds(pl.multiple_of(m * 2 * LANES, 2 * LANES), 2 * LANES)
            out = lax.dot_general(
                cot_all[source], w[rows, :], (((1,), (1,)), ((), ())), preferred_element_type=f32
            ).astype(bf16)
            ga_send[slot, 2 * m] = out[:, :LANES]
            ga_send[slot, 2 * m + 1] = out[:, LANES:]
            return _

        lax.fori_loop(0, cpd // 2, pair, 0)

    mine = pl.ds(d * cpd, cpd)
    project(d, 0)
    ga[mine] = ga_send[0]
    arrived(cot_all.at[partner], ids["partner"])
    project(partner, 1)
    send(ga_send.at[1], ga.at[mine], ids["ga"] + 1, s, partner)
    relay()
    for j in range(1, N // 2):
        origin = lax.rem(d + N - 2 * j, N)
        project(origin, 2 * j)
        send(ga_send.at[2 * j], ga.at[mine], ids["ga"] + 2 * j, s, origin)
    for j in range(1, N // 2):
        origin = lax.rem(partner + N - 2 * j, N)
        for h in range(HALVES):
            arrived(cot_all.at[origin, pl.ds(h * hrows, hrows)], ids["relay"] + j * HALVES + h)
        project(origin, 2 * j + 1)
        send(ga_send.at[2 * j + 1], ga.at[mine], ids["ga"] + 2 * j + 1, s, origin)

    for j in range(1, N):
        arrived(act_all.at[lax.rem(d + N - j, N)], ids["act"] + j)
    NT = min(C, 512)

    def weight_tile(i, _):
        m, n = i // (C // NT), lax.rem(i, C // NT)
        cols = pl.ds(pl.multiple_of(n * NT, NT), NT)
        acc = jnp.zeros((LANES, NT), f32)
        for q in range(N):
            acc = acc + lax.dot_general(
                act_all[q, m], cot_all[q, :, cols], (((0,), (0,)), ((), ())),
                preferred_element_type=f32,
            )
        wpart[pl.ds(pl.multiple_of(m * LANES, LANES), LANES), cols] = acc.astype(bf16)
        return _

    lax.fori_loop(0, cpd * (C // NT), weight_tile, 0)

    def block_of(j):
        i = lax.rem(s + j, S)
        owner = d * S + i
        rows = pl.ds(pl.multiple_of(i * block, block), block)
        return owner, rows, pltpu.make_async_remote_copy(
            src_ref=wpart.at[rows], dst_ref=rbuf.at[s], send_sem=send_sem.at[ids["rs"] + j],
            recv_sem=recv_sem.at[ids["rs"] + s],
            device_id={"sp": owner // N, "dp": lax.rem(owner, N)},
            device_id_type=pl.DeviceIdType.MESH,
        )

    def send_blocks(first, last):
        for j in range(first, last):
            owner, rows, c = block_of(j)

            @pl.when(owner != me)
            def _():
                c.start()

            @pl.when(owner == me)
            def _():
                rbuf[s] = wpart[rows, :]

    send_blocks(0, S // 2)

    for j in range(1, N // 2):
        arrived(ga.at[pl.ds(lax.rem(d + 2 * j, N) * cpd, cpd)], ids["ga"] + 2 * j)
        arrived(ga.at[pl.ds(lax.rem(partner + 2 * j, N) * cpd, cpd)], ids["ga"] + 2 * j + 1)
    arrived(ga.at[pl.ds(partner * cpd, cpd)], ids["ga"] + 1)

    def grad_chunk(cb, sums):
        one, two = sums
        centred = cen[cb]
        gain = kall[cb].astype(f32)[K : K + 1]
        normed = centred * gain
        sg = jax.nn.sigmoid(normed)
        grad = ga[cb].astype(f32) * sg * (1.0 + normed * (1.0 - sg))
        kg[cb, pl.ds(K, 1), :] = jnp.sum(grad * centred, axis=0, keepdims=True)
        grad = grad * gain
        gc[cb] = grad
        return one + grad, two + grad * centred

    zero = jnp.zeros((T, LANES), f32)
    one, two = lax.fori_loop(0, chunks, grad_chunk, (zero, zero))
    first = jnp.sum(one, axis=1, keepdims=True) / C
    second = jnp.sum(two, axis=1, keepdims=True) / C

    def conv_grad(cb, _):
        gext[cb, pl.ds(0, T), :] = (gc[cb] - first - cen[cb] * second) * inv
        return _

    lax.fori_loop(0, chunks, conv_grad, 0)
    send(gext.at[:, pl.ds(0, HB), :], gext.at[:, pl.ds(T, HB), :], ids["back"], preceding, d)

    def taps_chunk(cb, _):
        for k in range(K):
            acc = jnp.zeros((8, LANES), f32)
            for rb in range(T // RB):
                prod = gext[cb, pl.ds(rb * RB, RB), :] * ext[cb, pl.ds(HB - k + rb * RB, RB), :]
                acc = acc + jnp.sum(prod.reshape(RB // 8, 8, LANES), axis=0)
            kg[cb, pl.ds(k, 1), :] = jnp.sum(acc, axis=0, keepdims=True)
        return _

    lax.fori_loop(0, chunks, taps_chunk, 0)
    for j in range(1, S):
        to = lax.rem(s + j, S)
        send(kg.at[pl.ds(to * cps, cps)], krecv.at[j], ids["kg"] + j, to, d)
    send_blocks(S // 2, S)

    arrived(gext.at[:, pl.ds(T, HB), :], ids["back"])

    @pl.when(s == S - 1)
    def _():
        gext[:, pl.ds(T, HB), :] = jnp.zeros((chunks, HB, LANES), f32)

    def gated_chunk(cb, _):
        cols = pl.ds(pl.multiple_of(cb * LANES, LANES), LANES)
        tf = kall[cb].astype(f32)
        for rb in range(T // RB):
            rows = pl.ds(rb * RB, RB)
            acc = jnp.zeros((RB, LANES), f32)
            for k in range(K):
                acc = acc + tf[k : k + 1] * gext[cb, pl.ds(k + rb * RB, RB), :]
            acc = acc.astype(bf16).astype(f32)
            sig = jax.nn.sigmoid(gate[rows, cols].astype(f32))
            gv[rows, cols] = (acc * sig).astype(bf16)
            gg[rows, cols] = (acc * val[rows, cols].astype(f32) * sig * (1.0 - sig)).astype(bf16)
        return _

    lax.fori_loop(0, chunks, gated_chunk, 0)

    acc = kg[pl.ds(s * cps, cps)]
    for j in range(1, S):
        arrived(krecv.at[j], ids["kg"] + j)
        acc = acc + krecv[j]
    ksum[...] = acc
    for j in range(1, N):
        send(ksum, k2recv.at[j], ids["k2"] + j, s, lax.rem(d + j, N))
    for j in range(1, N):
        arrived(k2recv.at[j], ids["k2"] + j)
        acc = acc + k2recv[j]
    for c in range(cps):
        cols = slice(c * LANES, (c + 1) * LANES)
        kout[:, cols] = (acc[c] * factor)[:K]
        gout[:, cols] = (acc[c] * factor)[K : K + 1]

    home = me // S
    for q in range(S):
        @pl.when(jnp.logical_or(q != s, home != d))
        def _():
            arrived(rbuf.at[q], ids["rs"] + q)

    def sum_tile(n, _):
        cols = pl.ds(pl.multiple_of(n * LANES, LANES), LANES)
        acc = rbuf[0, :, cols].astype(f32)
        for q in range(1, S):
            acc = acc + rbuf[q, :, cols].astype(f32)
        gw[:, cols] = acc * factor
        return _

    lax.fori_loop(0, chunks, sum_tile, 0)
    for j in range(S):
        owner, rows, c = block_of(j)

        @pl.when(owner != me)
        def _():
            c.wait_send()

    for c in waits:
        c.wait_send()


def shards(out_cotangent, value_pre, gate_pre, out_weight, conv_kernel, norm_gain):
    S, N = lax.axis_size("sp"), lax.axis_size("dp")
    _, T, C = out_cotangent.shape
    K = conv_kernel.shape[0]
    chunks, cps, cpd, block = C // LANES, C // LANES // S, C // LANES // N, C // (S * N)
    HB = -(-(K - 1) // 16) * 16
    KP = -(-(K + 1) // 16) * 16
    packed = jnp.concatenate(
        [conv_kernel, norm_gain[None], jnp.zeros((KP - K - 1, C // S), bf16)], axis=0
    )
    packed = jnp.transpose(packed.reshape(KP, cps, LANES), (1, 0, 2))
    ids, count = {}, 0
    for name, size in (
        ("taps", S), ("front", 1), ("back", 1), ("partner", 1), ("mirror", N // 2 * HALVES),
        ("relay", N // 2 * HALVES), ("act", N), ("ga", N), ("rs", S), ("kg", S), ("k2", N),
    ):
        ids[name] = count
        count += size
    vm = pl.BlockSpec(memory_space=pltpu.VMEM)
    grad_value, grad_gate, grad_weight, grad_taps, grad_gain = pl.pallas_call(
        functools.partial(block_kernel, S, N, T, C, K, HB, ids),
        out_shape=(
            jax.ShapeDtypeStruct((T, C), bf16),
            jax.ShapeDtypeStruct((T, C), bf16),
            jax.ShapeDtypeStruct((block, C), f32),
            jax.ShapeDtypeStruct((K, C // S), f32),
            jax.ShapeDtypeStruct((1, C // S), f32),
        ),
        in_specs=[vm] * 5,
        out_specs=(vm,) * 5,
        scratch_shapes=[
            pltpu.VMEM((N, T, C), bf16),
            pltpu.VMEM((chunks, T + HB, LANES), f32),
            pltpu.VMEM((chunks, T, LANES), f32),
            pltpu.VMEM((chunks, T, LANES), f32),
            pltpu.VMEM((chunks, T + HB, LANES), f32),
            pltpu.VMEM((chunks, KP, LANES), bf16),
            pltpu.VMEM((chunks, T, LANES), bf16),
            pltpu.VMEM((N, cpd, T, LANES), bf16),
            pltpu.VMEM((N, cpd, T, LANES), bf16),
            pltpu.VMEM((chunks, T, LANES), bf16),
            pltpu.VMEM((cpd * LANES, C), bf16),
            pltpu.VMEM((S, block, C), bf16),
            pltpu.VMEM((chunks, KP, LANES), f32),
            pltpu.VMEM((S, cps, KP, LANES), f32),
            pltpu.VMEM((cps, KP, LANES), f32),
            pltpu.VMEM((N, cps, KP, LANES), f32),
            pltpu.SemaphoreType.DMA((count,)),
            pltpu.SemaphoreType.DMA((count,)),
        ],
        compiler_params=pltpu.CompilerParams(
            collective_id=0, has_side_effects=True, vmem_limit_bytes=60 * 1024 * 1024
        ),
        name="block_backward",
    )(out_cotangent[0], value_pre[0], gate_pre[0], out_weight, packed)
    return grad_value[None], grad_gate[None], grad_weight, grad_taps, grad_gain[0]


def solution(mesh):
    placed = (
        P("dp", "sp", None),
        P("dp", "sp", None),
        P("dp", "sp", None),
        P("dp", None),
        P(None, "sp"),
        P("sp"),
    )
    return jax.shard_map(
        shards,
        mesh=mesh,
        in_specs=placed,
        out_specs=(
            P("dp", "sp", None),
            P("dp", "sp", None),
            P(("sp", "dp"), None),
            P(None, "sp"),
            P("sp"),
        ),
        check_vma=False,
    )
```

profile of v0, /device:TPU:3, one launch (start us, length us, event | category | flops | bytes accessed | tf_op | source)
XLA Modules:
  0.0 157.8 jit_solution(13228991260276887878)
XLA Ops:
  0.6 0.7 copy.12
  1.3 0.7 concatenate.8
  2.0 0.6 maximum_bitcast_fusion.taps
  2.7 149.8 %block_backward.1 = (bf16[256,2048]{1,0:T(8,128)(2,1)}, bf16[256,2048]{1,0:T(8,128)(2,1)}, f32[64,2048]{1,0:T(8,128)}, f32[31,256]{1,0:T(8,128)}, f32[1,256]{1,0:T(1,128)}) custom-call(bf16[256,2048]{1,0:T(8,128)(2,1)} %bitcast.9, bf16[256,2048]{1,0:T(8,128)(2,1)} %bitcast.10, bf16[256,2048]{1,0:T(8,128)(2,1)} %bitcast.11, bf16[512,2048]{1,0:T(8,128)(2,1)} %w.1, ...), custom_call_target="tpu_custom_call" | custom-call | tf_op jit(solution)/shard_map/block_backward/pallas_call | solution.py:333
  152.4 0.0 copy-start
  152.4 0.0 copy-start.1
  152.5 2.4 %copy.18 = bf16[1,256,2048]{2,1,0:T(8,128)(2,1)} copy(bf16[1,256,2048]{2,1,0:T(8,128)(2,1)} %bitcast.13) | data formatting | bytes 2097152
  154.9 0.0 copy-done
  154.9 0.0 copy-start.2
  154.9 0.0 copy-start.3
  154.9 1.0 copy.19
  155.9 0.0 copy-done.1
  155.9 0.8 copy.20
  156.7 0.0 copy-done.2
  156.7 0.6 copy.21
  157.3 0.0 copy-done.3
  157.3 0.6 copy.22
  (1 shorter events, 0.0 us)
Async XLA Ops:
  152.4 2.4 %copy-start = (bf16[256,2048]{1,0:T(8,128)(2,1)S(1)}, bf16[256,2048]{1,0:T(8,128)(2,1)}, u32[]{:S(2)}) copy-start(bf16[256,2048]{1,0:T(8,128)(2,1)} %get-tuple-element.11) | copy-start | bytes 3145732
  152.4 3.4 %copy-start.1 = (f32[64,2048]{1,0:T(8,128)S(1)}, f32[64,2048]{1,0:T(8,128)}, u32[]{:S(2)}) copy-start(f32[64,2048]{1,0:T(8,128)} %get-tuple-element.22) | copy-start | bytes 1572868
  154.9 1.8 %copy-start.2 = (f32[31,256]{1,0:T(8,128)S(1)}, f32[31,256]{1,0:T(8,128)}, u32[]{:S(2)}) copy-start(f32[31,256]{1,0:T(8,128)} %get-tuple-element.23) | copy-start | bytes 95236
  154.9 2.4 %copy-start.3 = (f32[1,256]{1,0:T(1,128)S(1)}, f32[1,256]{1,0:T(1,128)}, u32[]{:S(2)}) copy-start(f32[1,256]{1,0:T(1,128)} %get-tuple-element.14) | copy-start | bytes 3076
where the time goes:
time: 158 us
  Pallas kernels  150 us (95%)
  local copies, waits for them, and re-layouts  6.78 us (4%)
    pallas_call x1, Pallas kernels, shards(): pl.pallas_call(functools.partial(block_kernel, S, N, T, C, K, HB, ids), o...  150 us
    unnamed x13, local copies, waits for them, and re-layouts  5.38 us

commit v1 on v0

--- a/solution.py
+++ b/solution.py
@@ -14,7 +14,7 @@
 bf16 = jnp.bfloat16
 
 
-def block_kernel(
+def general_kernel(
     S, N, T, C, K, HB, ids,
     cot, val, gate, w, taps,
     gv, gg, gw, kout, gout,
@@ -311,27 +311,521 @@
         c.wait_send()
 
 
-def shards(out_cotangent, value_pre, gate_pre, out_weight, conv_kernel, norm_gain):
-    S, N = lax.axis_size("sp"), lax.axis_size("dp")
-    _, T, C = out_cotangent.shape
-    K = conv_kernel.shape[0]
+def pair_kernel(
+    S, N, Y, T, C, K, HB, ids,
+    cot_in, val_in, gate_in, w_in, taps,
+    gv_out, gg_out, gw, kout, gout,
+    cot, val, gate, w, w_p, cot_m, cot_p, fsend, frecv, bsend, brecv, ext, cen, gc, gext, kall,
+    act, act_m, act_p, ga_s, ga, wacc, wpart, yrecv, ysum, zrecv, fin, fbuf, gv, gg,
+    kg, krecv, ksum, k2recv, send_sem, recv_sem, load_sem, store_sem,
+):
+    s = lax.axis_index("sp")
+    d = lax.axis_index("dp")
+    X, Z, H = N // 2, S // Y, C // 2
+    x, c = d // 2, lax.rem(d, 2)
+    y, z = lax.rem(s, Y), s // Y
+    other = 1 - c
+    partner = d + 1 - 2 * c
+    chunks = C // LANES
+    cps = chunks // S
+    cpd = chunks // N
+    block = C // (S * N)
+    M = chunks // X
+    RB = min(T, 128)
+    PT = T // HALVES
+    factor = float(S * N * T) ** (-0.5)
+    waits = []
+
+    def copy(src, dst, i, to_s, to_d, j=None):
+        return pltpu.make_async_remote_copy(
+            src_ref=src, dst_ref=dst, send_sem=send_sem.at[i],
+            recv_sem=recv_sem.at[i if j is None else j],
+            device_id={"sp": to_s, "dp": to_d}, device_id_type=pl.DeviceIdType.MESH,
+        )
+
+    def send(src, dst, i, to_s, to_d, j=None):
+        r = copy(src, dst, i, to_s, to_d, j)
+        r.start()
+        waits.append(r)
+
+    def arrived(dst, i):
+        copy(dst, dst, i, s, partner).wait_recv()
+
+    loads = [
+        pltpu.make_async_copy(a, b, load_sem.at[i])
+        for i, (a, b) in enumerate(((gate_in, gate), (val_in, val), (cot_in, cot), (w_in, w)))
+    ]
+    for l in loads:
+        l.start()
+
+    barrier = pltpu.get_barrier_semaphore()
+
+    def greet_s(j, _):
+        pl.semaphore_signal(
+            barrier, inc=1, device_id={"sp": lax.rem(s + j, S), "dp": d},
+            device_id_type=pl.DeviceIdType.MESH,
+        )
+        return _
+
+    def greet_d(j, _):
+        pl.semaphore_signal(
+            barrier, inc=1, device_id={"sp": s, "dp": lax.rem(d + j, N)},
+            device_id_type=pl.DeviceIdType.MESH,
+        )
+        return _
+
+    lax.fori_loop(1, N, greet_d, 0)
+    lax.fori_loop(1, S, greet_s, 0)
+    loads[0].wait()
+    loads[1].wait()
+
+    def gate_chunk(cb, _):
+        cols = pl.ds(pl.multiple_of(cb * LANES, LANES), LANES)
+        sig = jax.nn.sigmoid(gate[:, cols].astype(f32))
+        gated = (val[:, cols].astype(f32) * sig).astype(bf16)
+        ext[cb, pl.ds(HB, T), :] = gated.astype(f32)
+        fsend[cb] = gated[T - HB :]
+        return _
+
+    with jax.named_scope("gate"):
+        lax.fori_loop(0, chunks, gate_chunk, 0)
+    loads[2].wait()
+    with jax.named_scope("barrierwait"):
+        pl.semaphore_wait(barrier, S + N - 2)
+
+    for j in range(1, S):
+        send(taps, kall.at[pl.ds(s * cps, cps)], ids["taps"] + j, lax.rem(s + j, S), d)
+    front = copy(fsend, frecv, ids["front"], lax.rem(s + 1, S), d)
+
+    @pl.when(s < S - 1)
+    def _():
+        front.start()
+
+    for j in range(1, X):
+        for h in range(HALVES):
+            rows = pl.ds(h * PT, PT)
+            send(
+                cot.at[rows], cot_m.at[j - 1, rows], ids["cot"] + j * HALVES + h,
+                s, lax.rem(d + 2 * j, N),
+            )
+    half = pl.ds(pl.multiple_of(c * H, LANES), H)
+    ohalf = pl.ds(pl.multiple_of(other * H, LANES), H)
+    loads[3].wait()
+    send(w, w_p, ids["w"], s, partner)
+    send(cot.at[:, ohalf], cot_p.at[0], ids["cotp"], s, partner)
+    kall[pl.ds(s * cps, cps)] = taps[...]
+
+    def project(rows_of, weights, out, base):
+        def pair(m, _):
+            rows = pl.ds(pl.multiple_of(m * 2 * LANES, 2 * LANES), 2 * LANES)
+            prod = lax.dot_general(
+                rows_of[...], weights[rows, :], (((1,), (1,)), ((), ())), preferred_element_type=f32
+            ).astype(bf16)
+            out[base + 2 * m] = prod[:, :LANES]
+            out[base + 2 * m + 1] = prod[:, LANES:]
+            return _
+
+        lax.fori_loop(0, cpd // 2, pair, 0)
+
+    with jax.named_scope("proj_own"):
+        project(cot, w, ga, d * cpd)
+    with jax.named_scope("tapswait"):
+        for j in range(1, S):
+            arrived(kall.at[pl.ds(lax.rem(s + S - j, S) * cps, cps)], ids["taps"] + j)
+
+        @pl.when(s > 0)
+        def _():
+            arrived(frecv, ids["front"])
+
+    @pl.when(s == 0)
+    def _():
+        ext[:, pl.ds(0, HB), :] = jnp.zeros((chunks, HB, LANES), f32)
+
+    @pl.when(s > 0)
+    def _():
+        ext[:, pl.ds(0, HB), :] = frecv[...].astype(f32)
+
+    def conv_chunk(cb, sums):
+        tf = kall[cb].astype(f32)
+        parts = []
+        for rb in range(T // RB):
+            acc = jnp.zeros((RB, LANES), f32)
+            for k in range(K):
+                acc = acc + tf[k : k + 1] * ext[cb, pl.ds(HB - k + rb * RB, RB), :]
+            cen[cb, pl.ds(rb * RB, RB), :] = acc
+            parts.append(jnp.sum(acc, axis=1, keepdims=True))
+        return sums + jnp.concatenate(parts, axis=0)
+
+    column = jnp.zeros((T, 1), f32)
+    with jax.named_scope("conv"):
+        mean = lax.fori_loop(0, chunks, conv_chunk, column) / C
+
+    def square_chunk(cb, sums):
+        dev = cen[cb] - mean
+        return sums + dev * dev
+
+    with jax.named_scope("square"):
+        squares = lax.fori_loop(0, chunks, square_chunk, jnp.zeros((T, LANES), f32))
+    inv = lax.rsqrt(jnp.sum(squares, axis=1, keepdims=True) / C + epsilon)
+
+    def act_chunk(cb, _):
+        centred = (cen[cb] - mean) * inv
+        cen[cb] = centred
+        normed = centred * kall[cb].astype(f32)[K : K + 1]
+        act[lax.rem(cb, X), cb // X] = (normed * jax.nn.sigmoid(normed)).astype(bf16)
+        return _
+
+    with jax.named_scope("act"):
+        lax.fori_loop(0, chunks, act_chunk, 0)
+    for j in range(1, X):
+        send(act.at[lax.rem(x + j, X)], act_m.at[j - 1], ids["act"] + j, s, lax.rem(d + 2 * j, N))
+    send(act.at[x], act_p.at[0], ids["actp"], s, partner)
+
+    with jax.named_scope("proj_p"):
+        arrived(w_p, ids["w"])
+        project(cot, w_p, ga, partner * cpd)
+
+    dims = (((0,), (0,)), ((), ()))
+    NT = min(H, 512)
+    tiles = H // NT
+
+    def dot(a, b):
+        return lax.dot_general(a, b, dims, preferred_element_type=f32)
+
+    def local_tile(i, _):
+        m, n = i // tiles, lax.rem(i, tiles)
+        cols = pl.ds(pl.multiple_of(n * NT, NT), NT)
+        own = pl.ds(pl.multiple_of(c * H + n * NT, NT), NT)
+        wacc[m, :, cols] = dot(act[x, m], cot[:, own]) + dot(act_p[0, m], cot_p[0, :, cols])
+        return _
+
+    with jax.named_scope("wlocalwait"):
+        arrived(cot_p.at[0], ids["cotp"])
+        arrived(act_p.at[0], ids["actp"])
+    with jax.named_scope("wlocal"):
+        lax.fori_loop(0, M * tiles, local_tile, 0)
+
+    for h in range(HALVES):
+        rows = pl.ds(h * PT, PT)
+        for j in range(1, X):
+            with jax.named_scope("cotwait"):
+                arrived(cot_m.at[j - 1, rows], ids["cot"] + j * HALVES + h)
+            send(
+                cot_m.at[j - 1, rows, ohalf], cot_p.at[j, rows], ids["cotp"] + j * HALVES + h,
+                s, partner,
+            )
+            with jax.named_scope("proj_m"):
+                piece = ga_s.at[j - 1, :, rows]
+                project(cot_m.at[j - 1, rows], w, piece, c * cpd)
+                project(cot_m.at[j - 1, rows], w_p, piece, other * cpd)
+            send(
+                piece, ga.at[pl.ds(x * 2 * cpd, 2 * cpd), rows], ids["ga"] + j * HALVES + h,
+                s, lax.rem(d + 2 * (X - j), N),
+            )
+
+    with jax.named_scope("actwait"):
+        for j in range(1, X):
+            arrived(act_m.at[j - 1], ids["act"] + j)
+            send(act_m.at[j - 1], act_p.at[j], ids["actp"] + j, s, partner)
+        for j in range(1, X):
+            arrived(act_p.at[j], ids["actp"] + j)
+            for h in range(HALVES):
+                arrived(cot_p.at[j, pl.ds(h * PT, PT)], ids["cotp"] + j * HALVES + h)
+
+    def remote_part(m, n):
+        cols = pl.ds(pl.multiple_of(n * NT, NT), NT)
+        own = pl.ds(pl.multiple_of(c * H + n * NT, NT), NT)
+        acc = wacc[m, :, cols]
+        for j in range(1, X):
+            acc = acc + dot(act_m[j - 1, m], cot_m[j - 1, :, own]) + dot(act_p[j, m], cot_p[j, :, cols])
+        return cols, acc
+
+    def plane(k):
+        return jnp.where(z < Z // 2, lax.rem(z + Z - 1 - k, Z), lax.rem(z + 1 + k, Z))
+
+    with jax.named_scope("wremote"):
+        for k in range(Z):
+            for j in range(1, Y):
+                to_y = lax.rem(y + j, Y)
+                m = plane(k) * Y + to_y
+                i = (j - 1) * Z + k
+
+                def send_tile(n, _):
+                    cols, acc = remote_part(m, n)
+                    wpart[i, :, cols] = acc.astype(bf16)
+                    return _
+
+                lax.fori_loop(0, tiles, send_tile, 0)
+                send(wpart.at[i], yrecv.at[i], ids["y"] + i, z * Y + to_y, d)
+
+        def own_tile(i, _):
+            m = (i // tiles) * Y + y
+            cols, acc = remote_part(m, lax.rem(i, tiles))
+            wacc[m, :, cols] = acc
+            return _
+
+        lax.fori_loop(0, Z * tiles, own_tile, 0)
+
+    def reduce_y(k):
+        with jax.named_scope("ywait%d" % k):
+            for j in range(1, Y):
+                arrived(yrecv.at[(j - 1) * Z + k], ids["y"] + (j - 1) * Z + k)
+        to_z = plane(k)
+        m = to_z * Y + y
+
+        def tile(n, _):
+            cols = pl.ds(pl.multiple_of(n * LANES, LANES), LANES)
+            acc = wacc[m, :, cols]
+            for j in range(1, Y):
+                acc = acc + yrecv[(j - 1) * Z + k, :, cols].astype(f32)
+            if k < Z - 1:
+                ysum[k, :, cols] = acc.astype(bf16)
+            else:
+                wacc[m, :, cols] = acc
+            return _
+
+        lax.fori_loop(0, H // LANES, tile, 0)
+        if k < Z - 1:
+            slot = lax.rem(z - to_z + Z, Z)
+            send(ysum.at[k], zrecv.at[slot - 1], ids["z"] + 1 + k, to_z * Y + y, d, ids["z"] + slot)
+
+    with jax.named_scope("gawait"):
+        for j in range(1, X):
+            for h in range(HALVES):
+                rows = pl.ds(h * PT, PT)
+                origin = lax.rem(x + j, X)
+                arrived(ga.at[pl.ds(origin * 2 * cpd, 2 * cpd), rows], ids["ga"] + j * HALVES + h)
+
+    def grad_chunk(cb, sums):
+        one, two = sums
+        centred = cen[cb]
+        gain = kall[cb].astype(f32)[K : K + 1]
+        normed = centred * gain
+        sg = jax.nn.sigmoid(normed)
+        grad = ga[cb].astype(f32) * sg * (1.0 + normed * (1.0 - sg))
+        kg[cb, pl.ds(K, 1), :] = jnp.sum(grad * centred, axis=0, keepdims=True)
+        grad = grad * gain
+        gc[cb] = grad
+        return one + grad, two + grad * centred
+
+    zero = jnp.zeros((T, LANES), f32)
+    with jax.named_scope("gradchunk"):
+        one, two = lax.fori_loop(0, chunks, grad_chunk, (zero, zero))
+    first = jnp.sum(one, axis=1, keepdims=True) / C
+    second = jnp.sum(two, axis=1, keepdims=True) / C
+
+    def conv_grad(cb, _):
+        grad = (gc[cb] - first - cen[cb] * second) * inv
+        gext[cb, pl.ds(0, T), :] = grad
+        bsend[cb] = grad[:HB].astype(bf16)
+        return _
+
+    with jax.named_scope("convgrad"):
+        lax.fori_loop(0, chunks, conv_grad, 0)
+    back = copy(bsend, brecv, ids["back"], lax.rem(s + S - 1, S), d)
+
+    @pl.when(s > 0)
+    def _():
+        back.start()
+
+    reduce_y(0)
+
+    def taps_chunk(cb, _):
+        for k in range(K):
+            acc = jnp.zeros((8, LANES), f32)
+            for rb in range(T // RB):
+                prod = gext[cb, pl.ds(rb * RB, RB), :] * ext[cb, pl.ds(HB - k + rb * RB, RB), :]
+                acc = acc + jnp.sum(prod.reshape(RB // 8, 8, LANES), axis=0)
+            kg[cb, pl.ds(k, 1), :] = jnp.sum(acc, axis=0, keepdims=True)
+        return _
+
+    with jax.named_scope("taps"):
+        lax.fori_loop(0, chunks, taps_chunk, 0)
+    for j in range(1, S):
+        to = lax.rem(s + j, S)
+        send(kg.at[pl.ds(to * cps, cps)], krecv.at[j], ids["kg"] + j, to, d)
+    for k in range(1, Z - 1):
+        reduce_y(k)
+
+    with jax.named_scope("backwait"):
+        @pl.when(s < S - 1)
+        def _():
+            arrived(brecv, ids["back"])
+
+    @pl.when(s == S - 1)
+    def _():
+        gext[:, pl.ds(T, HB), :] = jnp.zeros((chunks, HB, LANES), f32)
+
+    @pl.when(s < S - 1)
+    def _():
+        gext[:, pl.ds(T, HB), :] = brecv[...].astype(f32)
+
+    stores = []
+    for rb in range(T // RB):
+        rows = pl.ds(rb * RB, RB)
+
+        def gated_chunk(cb, _):
+            cols = pl.ds(pl.multiple_of(cb * LANES, LANES), LANES)
+            tf = kall[cb].astype(f32)
+            acc = jnp.zeros((RB, LANES), f32)
+            for k in range(K):
+                acc = acc + tf[k : k + 1] * gext[cb, pl.ds(k + rb * RB, RB), :]
+            acc = acc.astype(bf16).astype(f32)
+            sig = jax.nn.sigmoid(gate[rows, cols].astype(f32))
+            gv[rows, cols] = (acc * sig).astype(bf16)
+            gg[rows, cols] = (acc * val[rows, cols].astype(f32) * sig * (1.0 - sig)).astype(bf16)
+            return _
+
+        with jax.named_scope("gated"):
+            lax.fori_loop(0, chunks, gated_chunk, 0)
+        for i, (a, b) in enumerate(((gv, gv_out), (gg, gg_out))):
+            st = pltpu.make_async_copy(a.at[rows], b.at[rows], store_sem.at[2 * rb + i])
+            st.start()
+            stores.append(st)
+
+    reduce_y(Z - 1)
+
+    with jax.named_scope("kgwait"):
+        for j in range(1, S):
+            arrived(krecv.at[j], ids["kg"] + j)
+    acc = kg[pl.ds(s * cps, cps)]
+    for j in range(1, S):
+        acc = acc + krecv[j]
+    ksum[...] = acc
+    for j in range(1, N):
+        send(ksum, k2recv.at[j], ids["k2"] + j, s, lax.rem(d + j, N))
+
+    with jax.named_scope("zwait"):
+        for j in range(1, Z):
+            arrived(zrecv.at[j - 1], ids["z"] + j)
+
+    def final_tile(n, _):
+        cols = pl.ds(pl.multiple_of(n * LANES, LANES), LANES)
+        acc = wacc[s, :, cols]
+        for j in range(1, Z):
+            acc = acc + zrecv[j - 1, :, cols].astype(f32)
+        acc = acc * factor
+        fin[0, :, cols] = acc[:block]
+        fin[1, :, cols] = acc[block:]
+        return _
+
+    with jax.named_scope("final"):
+        lax.fori_loop(0, H // LANES, final_tile, 0)
+    send(fin.at[other], fbuf, ids["fin"], s, partner)
+    gw[:, half] = fin[c]
+
+    with jax.named_scope("k2wait"):
+        for j in range(1, N):
+            arrived(k2recv.at[j], ids["k2"] + j)
+            acc = acc + k2recv[j]
+    for q in range(cps):
+        cols = slice(q * LANES, (q + 1) * LANES)
+        kout[:, cols] = (acc[q] * factor)[:K]
+        gout[:, cols] = (acc[q] * factor)[K : K + 1]
+
+    arrived(fbuf, ids["fin"])
+    gw[:, ohalf] = fbuf[...]
+    for r in waits:
+        r.wait_send()
+
+    @pl.when(s < S - 1)
+    def _():
+        front.wait_send()
+
+    @pl.when(s > 0)
+    def _():
+        back.wait_send()
+
+    for st in stores:
+        st.wait()
+
+
+def number(*sizes):
+    ids, count = {}, 0
+    for name, size in sizes:
+        ids[name] = count
+        count += size
+    return ids, count
+
+
+def pair_call(S, N, Y, T, C, K, HB, KP, cot, val, gate, w, packed):
+    X, Z, H = N // 2, S // Y, C // 2
     chunks, cps, cpd, block = C // LANES, C // LANES // S, C // LANES // N, C // (S * N)
-    HB = -(-(K - 1) // 16) * 16
-    KP = -(-(K + 1) // 16) * 16
-    packed = jnp.concatenate(
-        [conv_kernel, norm_gain[None], jnp.zeros((KP - K - 1, C // S), bf16)], axis=0
+    M, CR = chunks // X, C // N
+    ids, count = number(
+        ("taps", S), ("front", 1), ("back", 1), ("w", 1), ("cot", X * HALVES), ("cotp", X * HALVES),
+        ("act", X), ("actp", X), ("ga", X * HALVES), ("y", (Y - 1) * Z), ("z", Z), ("fin", 1),
+        ("kg", S), ("k2", N),
     )
-    packed = jnp.transpose(packed.reshape(KP, cps, LANES), (1, 0, 2))
-    ids, count = {}, 0
-    for name, size in (
+    vm = pl.BlockSpec(memory_space=pltpu.VMEM)
+    hbm = pl.BlockSpec(memory_space=pl.ANY)
+    return pl.pallas_call(
+        functools.partial(pair_kernel, S, N, Y, T, C, K, HB, ids),
+        out_shape=(
+            jax.ShapeDtypeStruct((T, C), bf16),
+            jax.ShapeDtypeStruct((T, C), bf16),
+            jax.ShapeDtypeStruct((block, C), f32),
+            jax.ShapeDtypeStruct((K, C // S), f32),
+            jax.ShapeDtypeStruct((1, C // S), f32),
+        ),
+        in_specs=[hbm] * 4 + [vm],
+        out_specs=(hbm, hbm, vm, vm, vm),
+        scratch_shapes=[
+            pltpu.VMEM((T, C), bf16),
+            pltpu.VMEM((T, C), bf16),
+            pltpu.VMEM((T, C), bf16),
+            pltpu.VMEM((CR, C), bf16),
+            pltpu.VMEM((CR, C), bf16),
+            pltpu.VMEM((X - 1, T, C), bf16),
+            pltpu.VMEM((X, T, H), bf16),
+            pltpu.VMEM((chunks, HB, LANES), bf16),
+            pltpu.VMEM((chunks, HB, LANES), bf16),
+            pltpu.VMEM((chunks, HB, LANES), bf16),
+            pltpu.VMEM((chunks, HB, LANES), bf16),
+            pltpu.VMEM((chunks, T + HB, LANES), f32),
+            pltpu.VMEM((chunks, T, LANES), f32),
+            pltpu.VMEM((chunks, T, LANES), f32),
+            pltpu.VMEM((chunks, T + HB, LANES), f32),
+            pltpu.VMEM((chunks, KP, LANES), bf16),
+            pltpu.VMEM((X, M, T, LANES), bf16),
+            pltpu.VMEM((X - 1, M, T, LANES), bf16),
+            pltpu.VMEM((X, M, T, LANES), bf16),
+            pltpu.VMEM((X - 1, 2 * cpd, T, LANES), bf16),
+            pltpu.VMEM((chunks, T, LANES), bf16),
+            pltpu.VMEM((M, LANES, H), f32),
+            pltpu.VMEM(((Y - 1) * Z, LANES, H), bf16),
+            pltpu.VMEM(((Y - 1) * Z, LANES, H), bf16),
+            pltpu.VMEM((Z - 1, LANES, H), bf16),
+            pltpu.VMEM((Z - 1, LANES, H), bf16),
+            pltpu.VMEM((2, block, H), f32),
+            pltpu.VMEM((block, H), f32),
+            pltpu.VMEM((T, C), bf16),
+            pltpu.VMEM((T, C), bf16),
+            pltpu.VMEM((chunks, KP, LANES), f32),
+            pltpu.VMEM((S, cps, KP, LANES), f32),
+            pltpu.VMEM((cps, KP, LANES), f32),
+            pltpu.VMEM((N, cps, KP, LANES), f32),
+            pltpu.SemaphoreType.DMA((count,)),
+            pltpu.SemaphoreType.DMA((count,)),
+            pltpu.SemaphoreType.DMA((4,)),
+            pltpu.SemaphoreType.DMA((2 * (T // min(T, 128)),)),
+        ],
+        compiler_params=pltpu.CompilerParams(
+            collective_id=0, has_side_effects=True, vmem_limit_bytes=62 * 1024 * 1024
+        ),
+        name="block_backward",
+    )(cot, val, gate, w, packed)
+
+
+def general_call(S, N, T, C, K, HB, KP, cot, val, gate, w, packed):
+    chunks, cps, cpd, block = C // LANES, C // LANES // S, C // LANES // N, C // (S * N)
+    ids, count = number(
         ("taps", S), ("front", 1), ("back", 1), ("partner", 1), ("mirror", N // 2 * HALVES),
         ("relay", N // 2 * HALVES), ("act", N), ("ga", N), ("rs", S), ("kg", S), ("k2", N),
-    ):
-        ids[name] = count
-        count += size
+    )
     vm = pl.BlockSpec(memory_space=pltpu.VMEM)
-    grad_value, grad_gate, grad_weight, grad_taps, grad_gain = pl.pallas_call(
-        functools.partial(block_kernel, S, N, T, C, K, HB, ids),
+    return pl.pallas_call(
+        functools.partial(general_kernel, S, N, T, C, K, HB, ids),
         out_shape=(
             jax.ShapeDtypeStruct((T, C), bf16),
             jax.ShapeDtypeStruct((T, C), bf16),
@@ -365,7 +859,27 @@
             collective_id=0, has_side_effects=True, vmem_limit_bytes=60 * 1024 * 1024
         ),
         name="block_backward",
-    )(out_cotangent[0], value_pre[0], gate_pre[0], out_weight, packed)
+    )(cot, val, gate, w, packed)
+
+
+def shards(out_cotangent, value_pre, gate_pre, out_weight, conv_kernel, norm_gain):
+    S, N = lax.axis_size("sp"), lax.axis_size("dp")
+    _, T, C = out_cotangent.shape
+    K = conv_kernel.shape[0]
+    chunks, cps = C // LANES, C // LANES // S
+    HB = -(-(K - 1) // 16) * 16
+    KP = -(-(K + 1) // 16) * 16
+    packed = jnp.concatenate(
+        [conv_kernel, norm_gain[None], jnp.zeros((KP - K - 1, C // S), bf16)], axis=0
+    )
+    packed = jnp.transpose(packed.reshape(KP, cps, LANES), (1, 0, 2))
+    args = (out_cotangent[0], value_pre[0], gate_pre[0], out_weight, packed)
+    X = N // 2
+    if N % 2 == 0 and X > 1 and S % X == 0 and S > X and chunks == S * X:
+        outs = pair_call(S, N, X, T, C, K, HB, KP, *args)
+    else:
+        outs = general_call(S, N, T, C, K, HB, KP, *args)
+    grad_value, grad_gate, grad_weight, grad_taps, grad_gain = outs
     return grad_value[None], grad_gate[None], grad_weight, grad_taps, grad_gain[0]
 
 

time: 158 us -> 98.2 us (0.62)
  the two profiles are of different devices: /device:TPU:3 before, /device:TPU:9 now
where the time goes in v1:
time: 98.2 us; the launch traced here: 97.8 us
  Pallas kernels  89.8 us (91%)
  local copies, waits for them, and re-layouts  6.78 us (7%)
    pallas_call x1, Pallas kernels, pair_call(): pl.pallas_call(functools.partial(pair_kernel, S, N, Y, T, C, K, HB, ids),...  89.8 us
    unnamed x13, local copies, waits for them, and re-layouts  5.38 us

profile of v1, /device:TPU:9, one launch (start us, length us, event | category | flops | bytes accessed | tf_op | source)
XLA Modules:
  0.0 97.8 jit_solution(8755038107752049996)
XLA Ops:
  0.6 0.7 copy.12
  1.3 0.7 concatenate.8
  2.0 0.6 maximum_bitcast_fusion.taps
  2.7 89.8 %block_backward.1 = (bf16[256,2048]{1,0:T(8,128)(2,1)}, bf16[256,2048]{1,0:T(8,128)(2,1)}, f32[64,2048]{1,0:T(8,128)}, f32[31,256]{1,0:T(8,128)}, f32[1,256]{1,0:T(1,128)}) custom-call(bf16[256,2048]{1,0:T(8,128)(2,1)} %bitcast.9, bf16[256,2048]{1,0:T(8,128)(2,1)} %bitcast.10, bf16[256,2048]{1,0:T(8,128)(2,1)} %bitcast.11, bf16[512,2048]{1,0:T(8,128)(2,1)} %w_in.1, ...), custom_call_target="tpu_custom_call" | custom-call | tf_op jit(solution)/shard_map/block_backward/pallas_call | solution.py:762
  92.4 0.0 copy-start
  92.5 0.0 copy-start.1
  92.5 2.4 %copy.18 = bf16[1,256,2048]{2,1,0:T(8,128)(2,1)} copy(bf16[1,256,2048]{2,1,0:T(8,128)(2,1)} %bitcast.13) | data formatting | bytes 2097152
  94.9 0.0 copy-done
  94.9 0.0 copy-start.2
  94.9 0.0 copy-start.3
  94.9 1.0 copy.19
  95.9 0.0 copy-done.1
  95.9 0.8 copy.20
  96.7 0.0 copy-done.2
  96.7 0.6 copy.21
  97.3 0.0 copy-done.3
  97.3 0.6 copy.22
  (1 shorter events, 0.0 us)
Async XLA Ops:
  92.4 2.4 %copy-start = (bf16[256,2048]{1,0:T(8,128)(2,1)S(1)}, bf16[256,2048]{1,0:T(8,128)(2,1)}, u32[]{:S(2)}) copy-start(bf16[256,2048]{1,0:T(8,128)(2,1)} %get-tuple-element.11) | copy-start | bytes 3145732
  92.5 3.4 %copy-start.1 = (f32[64,2048]{1,0:T(8,128)S(1)}, f32[64,2048]{1,0:T(8,128)}, u32[]{:S(2)}) copy-start(f32[64,2048]{1,0:T(8,128)} %get-tuple-element.22) | copy-start | bytes 1572868
  94.9 1.8 %copy-start.2 = (f32[31,256]{1,0:T(8,128)S(1)}, f32[31,256]{1,0:T(8,128)}, u32[]{:S(2)}) copy-start(f32[31,256]{1,0:T(8,128)} %get-tuple-element.23) | copy-start | bytes 95236
  94.9 2.4 %copy-start.3 = (f32[1,256]{1,0:T(1,128)S(1)}, f32[1,256]{1,0:T(1,128)}, u32[]{:S(2)}) copy-start(f32[1,256]{1,0:T(1,128)} %get-tuple-element.14) | copy-start | bytes 3076

commit v2 on v1

--- a/solution.py
+++ b/solution.py
@@ -10,6 +10,7 @@
 epsilon = 1e-05
 LANES = 128
 HALVES = 2
+BLOCKS = 4
 f32 = jnp.float32
 bf16 = jnp.bfloat16
 
@@ -313,11 +314,11 @@
 
 def pair_kernel(
     S, N, Y, T, C, K, HB, ids,
-    cot_in, val_in, gate_in, w_in, taps,
-    gv_out, gg_out, gw, kout, gout,
-    cot, val, gate, w, w_p, cot_m, cot_p, fsend, frecv, bsend, brecv, ext, cen, gc, gext, kall,
-    act, act_m, act_p, ga_s, ga, wacc, wpart, yrecv, ysum, zrecv, fin, fbuf, gv, gg,
-    kg, krecv, ksum, k2recv, send_sem, recv_sem, load_sem, store_sem,
+    cot_in, val_in, gate_in, w_in, kernel, gain,
+    gv_out, gg_out, gw, kout,
+    taps, cot, val, gate, w, w_p, cot_m, cot_p, fsend, frecv, bsend, brecv, ext, cen, gc, gext, kall,
+    act, act_m, act_p, ga_s, ga, wacc, wpart, yrecv, ysum, zmid, zrecv, fin, fbuf, gv, gg,
+    invs, kacc, kg, kgb, krecv, ksum, k2recv, send_sem, recv_sem, load_sem, store_sem, ready,
 ):
     s = lax.axis_index("sp")
     d = lax.axis_index("dp")
@@ -332,7 +333,7 @@
     block = C // (S * N)
     M = chunks // X
     RB = min(T, 128)
-    PT = T // HALVES
+    TB = T // BLOCKS
     factor = float(S * N * T) ** (-0.5)
     waits = []
 
@@ -360,22 +361,34 @@
 
     barrier = pltpu.get_barrier_semaphore()
 
-    def greet_s(j, _):
+    def signal(sem, to_s, to_d):
         pl.semaphore_signal(
-            barrier, inc=1, device_id={"sp": lax.rem(s + j, S), "dp": d},
-            device_id_type=pl.DeviceIdType.MESH,
+            sem, inc=1, device_id={"sp": to_s, "dp": to_d}, device_id_type=pl.DeviceIdType.MESH
         )
-        return _
-
-    def greet_d(j, _):
-        pl.semaphore_signal(
-            barrier, inc=1, device_id={"sp": s, "dp": lax.rem(d + j, N)},
-            device_id_type=pl.DeviceIdType.MESH,
-        )
-        return _
-
-    lax.fori_loop(1, N, greet_d, 0)
-    lax.fori_loop(1, S, greet_s, 0)
+
+    def along_z(action):
+        @pl.when(z > 0)
+        def _():
+            action(0, s - Y)
+
+        @pl.when(z < Z - 1)
+        def _():
+            action(1, s + Y)
+
+    signal(barrier, s, partner)
+    for j in range(1, X):
+        signal(barrier, s, lax.rem(d + 2 * j, N))
+    for j in range(1, Y):
+        signal(barrier, z * Y + lax.rem(y + j, Y), d)
+    along_z(lambda side, to_s: signal(barrier, to_s, d))
+    KP = taps.shape[1]
+    for q in range(cps):
+        cols = slice(q * LANES, (q + 1) * LANES)
+        taps[q] = jnp.concatenate(
+            [kernel[:, cols].astype(f32), gain[cols].astype(f32).reshape(1, LANES)]
+            + [jnp.zeros((KP - K - 1, LANES), f32)] * (KP > K + 1),
+            axis=0,
+        ).astype(bf16)
     loads[0].wait()
     loads[1].wait()
 
@@ -391,21 +404,13 @@
         lax.fori_loop(0, chunks, gate_chunk, 0)
     loads[2].wait()
     with jax.named_scope("barrierwait"):
-        pl.semaphore_wait(barrier, S + N - 2)
-
-    for j in range(1, S):
-        send(taps, kall.at[pl.ds(s * cps, cps)], ids["taps"] + j, lax.rem(s + j, S), d)
-    front = copy(fsend, frecv, ids["front"], lax.rem(s + 1, S), d)
-
-    @pl.when(s < S - 1)
-    def _():
-        front.start()
+        pl.semaphore_wait(barrier, X + Y - 1 + jnp.where(z > 0, 1, 0) + jnp.where(z < Z - 1, 1, 0))
 
     for j in range(1, X):
-        for h in range(HALVES):
-            rows = pl.ds(h * PT, PT)
+        for b in range(BLOCKS):
+            rows = pl.ds(b * TB, TB)
             send(
-                cot.at[rows], cot_m.at[j - 1, rows], ids["cot"] + j * HALVES + h,
+                cot.at[rows], cot_m.at[j - 1, rows], ids["cot"] + j * BLOCKS + b,
                 s, lax.rem(d + 2 * j, N),
             )
     half = pl.ds(pl.multiple_of(c * H, LANES), H)
@@ -414,6 +419,21 @@
     send(w, w_p, ids["w"], s, partner)
     send(cot.at[:, ohalf], cot_p.at[0], ids["cotp"], s, partner)
     kall[pl.ds(s * cps, cps)] = taps[...]
+    with jax.named_scope("ready"):
+        for r in range(Z - 2):
+            along_z(lambda side, to_s: signal(ready.at[2 * r + 1 - side], to_s, d))
+            along_z(lambda side, to_s: pl.semaphore_wait(ready.at[2 * r + side], 1))
+        for j in range(1, Y):
+            signal(ready.at[2 * (Z - 2)], z * Y + lax.rem(y + j, Y), d)
+        pl.semaphore_wait(ready.at[2 * (Z - 2)], Y - 1)
+    for j in range(1, S):
+        send(taps, kall.at[pl.ds(s * cps, cps)], ids["taps"] + j, lax.rem(s + j, S), d)
+    front = copy(fsend, frecv, ids["front"], lax.rem(s + 1, S), d)
+
+    @pl.when(s < S - 1)
+    def _():
+        front.start()
+
 
     def project(rows_of, weights, out, base):
         def pair(m, _):
@@ -477,60 +497,71 @@
 
     with jax.named_scope("act"):
         lax.fori_loop(0, chunks, act_chunk, 0)
-    for j in range(1, X):
-        send(act.at[lax.rem(x + j, X)], act_m.at[j - 1], ids["act"] + j, s, lax.rem(d + 2 * j, N))
+    invs[...] = jnp.broadcast_to(inv, (T, LANES))
     send(act.at[x], act_p.at[0], ids["actp"], s, partner)
 
-    with jax.named_scope("proj_p"):
-        arrived(w_p, ids["w"])
-        project(cot, w_p, ga, partner * cpd)
-
-    dims = (((0,), (0,)), ((), ()))
-    NT = min(H, 512)
-    tiles = H // NT
-
-    def dot(a, b):
-        return lax.dot_general(a, b, dims, preferred_element_type=f32)
-
-    def local_tile(i, _):
-        m, n = i // tiles, lax.rem(i, tiles)
-        cols = pl.ds(pl.multiple_of(n * NT, NT), NT)
-        own = pl.ds(pl.multiple_of(c * H + n * NT, NT), NT)
-        wacc[m, :, cols] = dot(act[x, m], cot[:, own]) + dot(act_p[0, m], cot_p[0, :, cols])
-        return _
-
-    with jax.named_scope("wlocalwait"):
-        arrived(cot_p.at[0], ids["cotp"])
-        arrived(act_p.at[0], ids["actp"])
-    with jax.named_scope("wlocal"):
-        lax.fori_loop(0, M * tiles, local_tile, 0)
-
-    for h in range(HALVES):
-        rows = pl.ds(h * PT, PT)
+    near = Z // 2
+    low = z < near
+    inner_z = jnp.where(low, near - 1, near)
+    inner = z == inner_z
+
+    def plane(k):
+        if k < near:
+            return jnp.where(low, Z - 1 - k, k)
+        return jnp.where(low, 0, near) + lax.rem(z + 1 + k, near)
+
+    def send_act(k):
+        piece = pl.ds(plane(k) * Y, Y)
         for j in range(1, X):
-            with jax.named_scope("cotwait"):
-                arrived(cot_m.at[j - 1, rows], ids["cot"] + j * HALVES + h)
             send(
-                cot_m.at[j - 1, rows, ohalf], cot_p.at[j, rows], ids["cotp"] + j * HALVES + h,
+                act.at[lax.rem(x + j, X), piece], act_m.at[j - 1, piece], ids["act"] + j * Z + k,
+                s, lax.rem(d + 2 * j, N),
+            )
+
+    def relay_mirror(b):
+        rows = pl.ds(b * TB, TB)
+        for j in range(1, X):
+            with jax.named_scope("cotwait%d" % b):
+                arrived(cot_m.at[j - 1, rows], ids["cot"] + j * BLOCKS + b)
+            send(
+                cot_m.at[j - 1, rows, ohalf], cot_p.at[j, rows], ids["cotp"] + j * BLOCKS + b,
                 s, partner,
             )
-            with jax.named_scope("proj_m"):
+
+    def project_mirror(b):
+        rows = pl.ds(b * TB, TB)
+        for j in range(1, X):
+            with jax.named_scope("proj_m%d" % b):
                 piece = ga_s.at[j - 1, :, rows]
                 project(cot_m.at[j - 1, rows], w, piece, c * cpd)
                 project(cot_m.at[j - 1, rows], w_p, piece, other * cpd)
             send(
-                piece, ga.at[pl.ds(x * 2 * cpd, 2 * cpd), rows], ids["ga"] + j * HALVES + h,
+                piece, ga.at[pl.ds(x * 2 * cpd, 2 * cpd), rows], ids["ga"] + j * BLOCKS + b,
                 s, lax.rem(d + 2 * (X - j), N),
             )
 
-    with jax.named_scope("actwait"):
-        for j in range(1, X):
-            arrived(act_m.at[j - 1], ids["act"] + j)
-            send(act_m.at[j - 1], act_p.at[j], ids["actp"] + j, s, partner)
-        for j in range(1, X):
-            arrived(act_p.at[j], ids["actp"] + j)
-            for h in range(HALVES):
-                arrived(cot_p.at[j, pl.ds(h * PT, PT)], ids["cotp"] + j * HALVES + h)
+    dims = (((0,), (0,)), ((), ()))
+    NT = min(H, 512)
+    tiles = H // NT
+
+    def dot(a, b):
+        return lax.dot_general(a, b, dims, preferred_element_type=f32)
+
+    def local_part(m, n):
+        cols = pl.ds(pl.multiple_of(n * NT, NT), NT)
+        own = pl.ds(pl.multiple_of(c * H + n * NT, NT), NT)
+        wacc[m, :, cols] = dot(act[x, m], cot[:, own]) + dot(act_p[0, m], cot_p[0, :, cols])
+
+    def local_plane(k):
+        def tile(i, _):
+            local_part(plane(k) * Y + i // tiles, lax.rem(i, tiles))
+            return _
+
+        with jax.named_scope("wlocal%d" % k):
+            if k == 0:
+                arrived(cot_p.at[0], ids["cotp"])
+                arrived(act_p.at[0], ids["actp"])
+            lax.fori_loop(0, Y * tiles, tile, 0)
 
     def remote_part(m, n):
         cols = pl.ds(pl.multiple_of(n * NT, NT), NT)
@@ -540,31 +571,36 @@
             acc = acc + dot(act_m[j - 1, m], cot_m[j - 1, :, own]) + dot(act_p[j, m], cot_p[j, :, cols])
         return cols, acc
 
-    def plane(k):
-        return jnp.where(z < Z // 2, lax.rem(z + Z - 1 - k, Z), lax.rem(z + 1 + k, Z))
-
-    with jax.named_scope("wremote"):
-        for k in range(Z):
+    def weight_plane(k):
+        piece = pl.ds(plane(k) * Y, Y)
+        with jax.named_scope("actwait%d" % k):
+            for j in range(1, X):
+                arrived(act_m.at[j - 1, piece], ids["act"] + j * Z + k)
+                send(act_m.at[j - 1, piece], act_p.at[j, piece], ids["actp"] + j * Z + k, s, partner)
+            for j in range(1, X):
+                arrived(act_p.at[j, piece], ids["actp"] + j * Z + k)
+                for b in range(BLOCKS if k == 0 else 0):
+                    arrived(cot_p.at[j, pl.ds(b * TB, TB)], ids["cotp"] + j * BLOCKS + b)
+        with jax.named_scope("wremote%d" % k):
             for j in range(1, Y):
                 to_y = lax.rem(y + j, Y)
-                m = plane(k) * Y + to_y
                 i = (j - 1) * Z + k
 
                 def send_tile(n, _):
-                    cols, acc = remote_part(m, n)
+                    cols, acc = remote_part(plane(k) * Y + to_y, n)
                     wpart[i, :, cols] = acc.astype(bf16)
                     return _
 
                 lax.fori_loop(0, tiles, send_tile, 0)
                 send(wpart.at[i], yrecv.at[i], ids["y"] + i, z * Y + to_y, d)
 
-        def own_tile(i, _):
-            m = (i // tiles) * Y + y
-            cols, acc = remote_part(m, lax.rem(i, tiles))
-            wacc[m, :, cols] = acc
-            return _
-
-        lax.fori_loop(0, Z * tiles, own_tile, 0)
+            def own_tile(n, _):
+                m = plane(k) * Y + y
+                cols, acc = remote_part(m, n)
+                wacc[m, :, cols] = acc
+                return _
+
+            lax.fori_loop(0, tiles, own_tile, 0)
 
     def reduce_y(k):
         with jax.named_scope("ywait%d" % k):
@@ -580,130 +616,206 @@
                 acc = acc + yrecv[(j - 1) * Z + k, :, cols].astype(f32)
             if k < Z - 1:
                 ysum[k, :, cols] = acc.astype(bf16)
-            else:
+            if k != Z - 2:
                 wacc[m, :, cols] = acc
             return _
 
         lax.fori_loop(0, H // LANES, tile, 0)
-        if k < Z - 1:
-            slot = lax.rem(z - to_z + Z, Z)
-            send(ysum.at[k], zrecv.at[slot - 1], ids["z"] + 1 + k, to_z * Y + y, d, ids["z"] + slot)
-
-    with jax.named_scope("gawait"):
-        for j in range(1, X):
-            for h in range(HALVES):
-                rows = pl.ds(h * PT, PT)
+        if k < near:
+            r = copy(ysum.at[k], zmid.at[k], ids["z"] + k, inner_z * Y + y, d)
+
+            @pl.when(jnp.logical_not(inner))
+            def _():
+                r.start()
+
+            outer.append(r)
+        elif k < Z - 1:
+            send(ysum.at[k], zrecv.at[0], ids["z"] + near, to_z * Y + y, d)
+
+    def reduce_z(k):
+        to_z = plane(k)
+        m = to_z * Y + y
+
+        def tile(n, _):
+            cols = pl.ds(pl.multiple_of(n * LANES, LANES), LANES)
+            ysum[k, :, cols] = (wacc[m, :, cols] + zmid[k, :, cols].astype(f32)).astype(bf16)
+            return _
+
+        r = copy(ysum.at[k], zrecv.at[1], ids["z"] + k, to_z * Y + y, d, ids["z"] + near + 1)
+
+        @pl.when(inner)
+        def _():
+            with jax.named_scope("zmid%d" % k):
+                arrived(zmid.at[k], ids["z"] + k)
+            lax.fori_loop(0, H // LANES, tile, 0)
+            r.start()
+
+    outer = []
+
+    def fold(v):
+        return jnp.sum(v.reshape(v.shape[0] // 8, 8, LANES), axis=0)
+
+    def gradient(b):
+        rows = pl.ds(b * TB, TB)
+        with jax.named_scope("gawait%d" % b):
+            for j in range(1, X):
                 origin = lax.rem(x + j, X)
-                arrived(ga.at[pl.ds(origin * 2 * cpd, 2 * cpd), rows], ids["ga"] + j * HALVES + h)
-
-    def grad_chunk(cb, sums):
-        one, two = sums
-        centred = cen[cb]
-        gain = kall[cb].astype(f32)[K : K + 1]
-        normed = centred * gain
-        sg = jax.nn.sigmoid(normed)
-        grad = ga[cb].astype(f32) * sg * (1.0 + normed * (1.0 - sg))
-        kg[cb, pl.ds(K, 1), :] = jnp.sum(grad * centred, axis=0, keepdims=True)
-        grad = grad * gain
-        gc[cb] = grad
-        return one + grad, two + grad * centred
-
-    zero = jnp.zeros((T, LANES), f32)
-    with jax.named_scope("gradchunk"):
-        one, two = lax.fori_loop(0, chunks, grad_chunk, (zero, zero))
-    first = jnp.sum(one, axis=1, keepdims=True) / C
-    second = jnp.sum(two, axis=1, keepdims=True) / C
-
-    def conv_grad(cb, _):
-        grad = (gc[cb] - first - cen[cb] * second) * inv
-        gext[cb, pl.ds(0, T), :] = grad
-        bsend[cb] = grad[:HB].astype(bf16)
-        return _
-
-    with jax.named_scope("convgrad"):
-        lax.fori_loop(0, chunks, conv_grad, 0)
-    back = copy(bsend, brecv, ids["back"], lax.rem(s + S - 1, S), d)
-
-    @pl.when(s > 0)
-    def _():
-        back.start()
-
-    reduce_y(0)
-
-    def taps_chunk(cb, _):
-        for k in range(K):
-            acc = jnp.zeros((8, LANES), f32)
-            for rb in range(T // RB):
-                prod = gext[cb, pl.ds(rb * RB, RB), :] * ext[cb, pl.ds(HB - k + rb * RB, RB), :]
-                acc = acc + jnp.sum(prod.reshape(RB // 8, 8, LANES), axis=0)
-            kg[cb, pl.ds(k, 1), :] = jnp.sum(acc, axis=0, keepdims=True)
-        return _
-
-    with jax.named_scope("taps"):
-        lax.fori_loop(0, chunks, taps_chunk, 0)
-    for j in range(1, S):
-        to = lax.rem(s + j, S)
-        send(kg.at[pl.ds(to * cps, cps)], krecv.at[j], ids["kg"] + j, to, d)
-    for k in range(1, Z - 1):
-        reduce_y(k)
-
-    with jax.named_scope("backwait"):
-        @pl.when(s < S - 1)
-        def _():
-            arrived(brecv, ids["back"])
-
-    @pl.when(s == S - 1)
-    def _():
-        gext[:, pl.ds(T, HB), :] = jnp.zeros((chunks, HB, LANES), f32)
-
-    @pl.when(s < S - 1)
-    def _():
-        gext[:, pl.ds(T, HB), :] = brecv[...].astype(f32)
+                arrived(ga.at[pl.ds(origin * 2 * cpd, 2 * cpd), rows], ids["ga"] + j * BLOCKS + b)
+
+        def grad_chunk(cb, sums):
+            one, two = sums
+            centred = cen[cb, rows, :]
+            gain = kall[cb].astype(f32)[K : K + 1]
+            normed = centred * gain
+            sg = jax.nn.sigmoid(normed)
+            grad = ga[cb, rows, :].astype(f32) * sg * (1.0 + normed * (1.0 - sg))
+            scaled = grad * centred
+            kacc[cb, K] = fold(scaled) if b == 0 else kacc[cb, K] + fold(scaled)
+            gc[cb, rows, :] = grad * gain
+            return one + grad * gain, two + scaled * gain
+
+        zero = jnp.zeros((TB, LANES), f32)
+        with jax.named_scope("gradchunk%d" % b):
+            one, two = lax.fori_loop(0, chunks, grad_chunk, (zero, zero))
+        first = jnp.sum(one, axis=1, keepdims=True) / C
+        second = jnp.sum(two, axis=1, keepdims=True) / C
+        scale = invs[rows, :]
+
+        def conv_grad(cb, _):
+            grad = (gc[cb, rows, :] - first - cen[cb, rows, :] * second) * scale
+            gext[cb, rows, :] = grad
+            if b == 0:
+                bsend[cb] = grad[:HB].astype(bf16)
+            return _
+
+        with jax.named_scope("convgrad%d" % b):
+            lax.fori_loop(0, chunks, conv_grad, 0)
+
+    def taps_grad(b):
+        def taps_chunk(cb, _):
+            grad = gext[cb, pl.ds(b * TB, TB), :]
+            for k in range(K):
+                acc = fold(grad * ext[cb, pl.ds(HB - k + b * TB, TB), :])
+                if b > 0:
+                    acc = acc + kacc[cb, k]
+                if b < BLOCKS - 1:
+                    kacc[cb, k] = acc
+                else:
+                    kg[cb, pl.ds(k, 1), :] = jnp.sum(acc, axis=0, keepdims=True)
+            if b == BLOCKS - 1:
+                kg[cb, pl.ds(K, 1), :] = jnp.sum(kacc[cb, K], axis=0, keepdims=True)
+                kgb[cb] = kg[cb].astype(bf16)
+            return _
+
+        with jax.named_scope("taps%d" % b):
+            lax.fori_loop(0, chunks, taps_chunk, 0)
 
     stores = []
-    for rb in range(T // RB):
-        rows = pl.ds(rb * RB, RB)
+
+    def gated_grad(b):
+        rows = pl.ds(b * TB, TB)
 
         def gated_chunk(cb, _):
             cols = pl.ds(pl.multiple_of(cb * LANES, LANES), LANES)
             tf = kall[cb].astype(f32)
-            acc = jnp.zeros((RB, LANES), f32)
+            acc = jnp.zeros((TB, LANES), f32)
             for k in range(K):
-                acc = acc + tf[k : k + 1] * gext[cb, pl.ds(k + rb * RB, RB), :]
+                acc = acc + tf[k : k + 1] * gext[cb, pl.ds(k + b * TB, TB), :]
             acc = acc.astype(bf16).astype(f32)
             sig = jax.nn.sigmoid(gate[rows, cols].astype(f32))
             gv[rows, cols] = (acc * sig).astype(bf16)
             gg[rows, cols] = (acc * val[rows, cols].astype(f32) * sig * (1.0 - sig)).astype(bf16)
             return _
 
-        with jax.named_scope("gated"):
+        with jax.named_scope("gated%d" % b):
             lax.fori_loop(0, chunks, gated_chunk, 0)
-        for i, (a, b) in enumerate(((gv, gv_out), (gg, gg_out))):
-            st = pltpu.make_async_copy(a.at[rows], b.at[rows], store_sem.at[2 * rb + i])
+        for i, (src, dst) in enumerate(((gv, gv_out), (gg, gg_out))):
+            st = pltpu.make_async_copy(src.at[rows], dst.at[rows], store_sem.at[2 * b + i])
             st.start()
             stores.append(st)
 
-    reduce_y(Z - 1)
-
+    back = copy(bsend, brecv, ids["back"], lax.rem(s + S - 1, S), d)
+    back = copy(bsend, brecv, ids["back"], lax.rem(s + S - 1, S), d)
+    arrived(w_p, ids["w"])
+    send_act(0)
+    send_act(1)
+    relay_mirror(0)
+    project_mirror(0)
+    send_act(2)
+    relay_mirror(1)
+    project_mirror(1)
+    send_act(3)
+    relay_mirror(2)
+    project_mirror(2)
+    local_plane(0)
+    relay_mirror(3)
+    with jax.named_scope("proj_p"):
+        project(cot, w_p, ga, partner * cpd)
+    weight_plane(0)
+    project_mirror(3)
+    for k in (1, 2):
+        local_plane(k)
+        weight_plane(k)
+    reduce_y(0)
+    gradient(0)
+
+    @pl.when(s > 0)
+    def _():
+        back.start()
+
+    taps_grad(0)
+    local_plane(3)
+    weight_plane(3)
+    gradient(1)
+    taps_grad(1)
+    reduce_y(1)
+    gradient(2)
+    taps_grad(2)
+    reduce_z(0)
+    gradient(3)
+    taps_grad(3)
+    for j in range(1, S):
+        to = lax.rem(s + j, S)
+        send(kgb.at[pl.ds(to * cps, cps)], krecv.at[j], ids["kg"] + j, to, d)
+    reduce_y(2)
+    gated_grad(0)
+    reduce_z(1)
+    gated_grad(1)
+    gated_grad(2)
+    with jax.named_scope("backwait"):
+        @pl.when(s < S - 1)
+        def _():
+            arrived(brecv, ids["back"])
+
+    @pl.when(s == S - 1)
+    def _():
+        gext[:, pl.ds(T, HB), :] = jnp.zeros((chunks, HB, LANES), f32)
+
+    @pl.when(s < S - 1)
+    def _():
+        gext[:, pl.ds(T, HB), :] = brecv[...].astype(f32)
+
+    gated_grad(3)
     with jax.named_scope("kgwait"):
         for j in range(1, S):
             arrived(krecv.at[j], ids["kg"] + j)
     acc = kg[pl.ds(s * cps, cps)]
     for j in range(1, S):
-        acc = acc + krecv[j]
+        acc = acc + krecv[j].astype(f32)
     ksum[...] = acc
     for j in range(1, N):
         send(ksum, k2recv.at[j], ids["k2"] + j, s, lax.rem(d + j, N))
 
+    reduce_y(3)
     with jax.named_scope("zwait"):
-        for j in range(1, Z):
-            arrived(zrecv.at[j - 1], ids["z"] + j)
+        for q in range(2):
+            arrived(zrecv.at[q], ids["z"] + near + q)
 
     def final_tile(n, _):
         cols = pl.ds(pl.multiple_of(n * LANES, LANES), LANES)
         acc = wacc[s, :, cols]
-        for j in range(1, Z):
-            acc = acc + zrecv[j - 1, :, cols].astype(f32)
+        for q in range(2):
+            acc = acc + zrecv[q, :, cols].astype(f32)
         acc = acc * factor
         fin[0, :, cols] = acc[:block]
         fin[1, :, cols] = acc[block:]
@@ -720,12 +832,11 @@
             acc = acc + k2recv[j]
     for q in range(cps):
         cols = slice(q * LANES, (q + 1) * LANES)
-        kout[:, cols] = (acc[q] * factor)[:K]
-        gout[:, cols] = (acc[q] * factor)[K : K + 1]
+        kout[:, cols] = acc[q] * factor
 
     arrived(fbuf, ids["fin"])
     gw[:, ohalf] = fbuf[...]
-    for r in waits:
+    for r in waits + outer:
         r.wait_send()
 
     @pl.when(s < S - 1)
@@ -748,29 +859,49 @@
     return ids, count
 
 
-def pair_call(S, N, Y, T, C, K, HB, KP, cot, val, gate, w, packed):
+def hand_over(K, gv_in, gg_in, gw_in, k_in, gv, gg, gw, kout, gout, a, b, c, sem):
+    T = gv_in.shape[0]
+    pieces = []
+    for n in range(2):
+        rows = pl.ds(n * (T // 2), T // 2)
+        pieces += [(gv_in.at[rows], a.at[rows], gv.at[rows]), (gg_in.at[rows], b.at[rows], gg.at[rows])]
+    pieces.append((gw_in, c, gw))
+    loads = [pltpu.make_async_copy(p[0], p[1], sem.at[0, i]) for i, p in enumerate(pieces)]
+    stores = [pltpu.make_async_copy(p[1], p[2], sem.at[1, i]) for i, p in enumerate(pieces)]
+    for l in loads:
+        l.start()
+    kout[...] = k_in[:K]
+    gout[...] = k_in[K : K + 1]
+    for l, st in zip(loads, stores):
+        l.wait()
+        st.start()
+    for st in stores:
+        st.wait()
+
+
+def pair_call(S, N, Y, T, C, K, HB, KP, cot, val, gate, w, kernel, gain):
     X, Z, H = N // 2, S // Y, C // 2
     chunks, cps, cpd, block = C // LANES, C // LANES // S, C // LANES // N, C // (S * N)
     M, CR = chunks // X, C // N
     ids, count = number(
-        ("taps", S), ("front", 1), ("back", 1), ("w", 1), ("cot", X * HALVES), ("cotp", X * HALVES),
-        ("act", X), ("actp", X), ("ga", X * HALVES), ("y", (Y - 1) * Z), ("z", Z), ("fin", 1),
+        ("taps", S), ("front", 1), ("back", 1), ("w", 1), ("cot", X * BLOCKS), ("cotp", X * BLOCKS),
+        ("act", X * Z), ("actp", X * Z), ("ga", X * BLOCKS), ("y", (Y - 1) * Z), ("z", Z // 2 + 2), ("fin", 1),
         ("kg", S), ("k2", N),
     )
     vm = pl.BlockSpec(memory_space=pltpu.VMEM)
     hbm = pl.BlockSpec(memory_space=pl.ANY)
-    return pl.pallas_call(
+    partial = pl.pallas_call(
         functools.partial(pair_kernel, S, N, Y, T, C, K, HB, ids),
         out_shape=(
             jax.ShapeDtypeStruct((T, C), bf16),
             jax.ShapeDtypeStruct((T, C), bf16),
             jax.ShapeDtypeStruct((block, C), f32),
-            jax.ShapeDtypeStruct((K, C // S), f32),
-            jax.ShapeDtypeStruct((1, C // S), f32),
+            jax.ShapeDtypeStruct((KP, C // S), f32),
         ),
-        in_specs=[hbm] * 4 + [vm],
-        out_specs=(hbm, hbm, vm, vm, vm),
+        in_specs=[hbm] * 4 + [vm] * 2,
+        out_specs=(hbm, hbm, vm, vm),
         scratch_shapes=[
+            pltpu.VMEM((cps, KP, LANES), bf16),
             pltpu.VMEM((T, C), bf16),
             pltpu.VMEM((T, C), bf16),
             pltpu.VMEM((T, C), bf16),
@@ -796,25 +927,49 @@
             pltpu.VMEM(((Y - 1) * Z, LANES, H), bf16),
             pltpu.VMEM(((Y - 1) * Z, LANES, H), bf16),
             pltpu.VMEM((Z - 1, LANES, H), bf16),
-            pltpu.VMEM((Z - 1, LANES, H), bf16),
+            pltpu.VMEM((Z // 2, LANES, H), bf16),
+            pltpu.VMEM((2, LANES, H), bf16),
             pltpu.VMEM((2, block, H), f32),
             pltpu.VMEM((block, H), f32),
             pltpu.VMEM((T, C), bf16),
             pltpu.VMEM((T, C), bf16),
+            pltpu.VMEM((T, LANES), f32),
+            pltpu.VMEM((chunks, K + 1, 8, LANES), f32),
             pltpu.VMEM((chunks, KP, LANES), f32),
-            pltpu.VMEM((S, cps, KP, LANES), f32),
+            pltpu.VMEM((chunks, KP, LANES), bf16),
+            pltpu.VMEM((S, cps, KP, LANES), bf16),
             pltpu.VMEM((cps, KP, LANES), f32),
             pltpu.VMEM((N, cps, KP, LANES), f32),
             pltpu.SemaphoreType.DMA((count,)),
             pltpu.SemaphoreType.DMA((count,)),
             pltpu.SemaphoreType.DMA((4,)),
-            pltpu.SemaphoreType.DMA((2 * (T // min(T, 128)),)),
+            pltpu.SemaphoreType.DMA((2 * BLOCKS,)),
+            pltpu.SemaphoreType.REGULAR((2 * (Z - 2) + 1,)),
         ],
         compiler_params=pltpu.CompilerParams(
             collective_id=0, has_side_effects=True, vmem_limit_bytes=62 * 1024 * 1024
         ),
         name="block_backward",
-    )(cot, val, gate, w, packed)
+    )(cot, val, gate, w, kernel, gain)
+    return pl.pallas_call(
+        functools.partial(hand_over, K),
+        out_shape=(
+            jax.ShapeDtypeStruct((T, C), bf16),
+            jax.ShapeDtypeStruct((T, C), bf16),
+            jax.ShapeDtypeStruct((block, C), f32),
+            jax.ShapeDtypeStruct((K, C // S), f32),
+            jax.ShapeDtypeStruct((1, C // S), f32),
+        ),
+        in_specs=[hbm] * 3 + [vm],
+        out_specs=(hbm, hbm, hbm, vm, vm),
+        scratch_shapes=[
+            pltpu.VMEM((T, C), bf16),
+            pltpu.VMEM((T, C), bf16),
+            pltpu.VMEM((block, C), f32),
+            pltpu.SemaphoreType.DMA((2, 5)),
+        ],
+        name="hand_over",
+    )(*partial)
 
 
 def general_call(S, N, T, C, K, HB, KP, cot, val, gate, w, packed):
@@ -869,16 +1024,16 @@
     chunks, cps = C // LANES, C // LANES // S
     HB = -(-(K - 1) // 16) * 16
     KP = -(-(K + 1) // 16) * 16
-    packed = jnp.concatenate(
-        [conv_kernel, norm_gain[None], jnp.zeros((KP - K - 1, C // S), bf16)], axis=0
-    )
-    packed = jnp.transpose(packed.reshape(KP, cps, LANES), (1, 0, 2))
-    args = (out_cotangent[0], value_pre[0], gate_pre[0], out_weight, packed)
+    args = (out_cotangent[0], value_pre[0], gate_pre[0], out_weight)
     X = N // 2
-    if N % 2 == 0 and X > 1 and S % X == 0 and S > X and chunks == S * X:
-        outs = pair_call(S, N, X, T, C, K, HB, KP, *args)
+    if N == 2 * X > 2 and S == 2 * 2 * X and chunks == S * X:
+        outs = pair_call(S, N, X, T, C, K, HB, KP, *args, conv_kernel, norm_gain)
     else:
-        outs = general_call(S, N, T, C, K, HB, KP, *args)
+        packed = jnp.concatenate(
+            [conv_kernel, norm_gain[None], jnp.zeros((KP - K - 1, C // S), bf16)], axis=0
+        )
+        packed = jnp.transpose(packed.reshape(KP, cps, LANES), (1, 0, 2))
+        outs = general_call(S, N, T, C, K, HB, KP, *args, packed)
     grad_value, grad_gate, grad_weight, grad_taps, grad_gain = outs
     return grad_value[None], grad_gate[None], grad_weight, grad_taps, grad_gain[0]
 

time: 98.2 us -> 78.7 us (0.80)
  the two profiles are of different devices: /device:TPU:9 before, /device:TPU:0 now
where the time goes in v2:
time: 78.7 us; the launch traced here: 78.4 us
  Pallas kernels  77.7 us (99%)
    pallas_call x1, Pallas kernels, pair_call(): pl.pallas_call(functools.partial(pair_kernel, S, N, Y, T, C, K, HB, ids),...  73.8 us
    pallas_call x1, Pallas kernels, pair_call(): pl.pallas_call(functools.partial(hand_over, K), out_shape=(jax.ShapeDtype...  3.99 us

profile of v2, /device:TPU:0, one launch (start us, length us, event | category | flops | bytes accessed | tf_op | source)
XLA Modules:
  0.0 78.4 jit_solution(17926992385863715925)
XLA Ops:
  0.6 73.8 %block_backward.1 = (bf16[256,2048]{1,0:T(8,128)(2,1)}, bf16[256,2048]{1,0:T(8,128)(2,1)}, f32[64,2048]{1,0:T(8,128)}, f32[32,256]{1,0:T(8,128)}) custom-call(bf16[256,2048]{1,0:T(8,128)(2,1)} %bitcast.6, bf16[256,2048]{1,0:T(8,128)(2,1)} %bitcast.7, bf16[256,2048]{1,0:T(8,128)(2,1)} %bitcast.8, bf16[512,2048]{1,0:T(8,128)(2,1)} %w_in.1, ...), custom_call_target="tpu_custom_call" | custom-call | tf_op jit(solution)/shard_map/block_backward/pallas_call | solution.py:893
  74.4 4.0 %hand_over.1 = (bf16[256,2048]{1,0:T(8,128)(2,1)}, bf16[256,2048]{1,0:T(8,128)(2,1)}, f32[64,2048]{1,0:T(8,128)}, f32[31,256]{1,0:T(8,128)}, f32[1,256]{1,0:T(1,128)}) custom-call(bf16[256,2048]{1,0:T(8,128)(2,1)} %get-tuple-element.14.gv_in, bf16[256,2048]{1,0:T(8,128)(2,1)} %get-tuple-element.15.gg_in, f32[64,2048]{1,0:T(8,128)} %get-tuple-element.16.gw_in, ...), custom_call_target="tpu_custom_call" | custom-call | tf_op jit(solution)/shard_map/hand_over/pallas_call | solution.py:954

commit v3 on v2

--- a/solution.py
+++ b/solution.py
@@ -318,7 +318,7 @@
     gv_out, gg_out, gw, kout,
     taps, cot, val, gate, w, w_p, cot_m, cot_p, fsend, frecv, bsend, brecv, ext, cen, gc, gext, kall,
     act, act_m, act_p, ga_s, ga, wacc, wpart, yrecv, ysum, zmid, zrecv, fin, fbuf, gv, gg,
-    invs, kacc, kg, kgb, krecv, ksum, k2recv, send_sem, recv_sem, load_sem, store_sem, ready,
+    means, invs, sum1, sum2, kacc, kg, kgb, krecv, ksum, k2recv, send_sem, recv_sem, load_sem, store_sem, ready,
 ):
     s = lax.axis_index("sp")
     d = lax.axis_index("dp")
@@ -406,13 +406,20 @@
     with jax.named_scope("barrierwait"):
         pl.semaphore_wait(barrier, X + Y - 1 + jnp.where(z > 0, 1, 0) + jnp.where(z < Z - 1, 1, 0))
 
-    for j in range(1, X):
-        for b in range(BLOCKS):
-            rows = pl.ds(b * TB, TB)
-            send(
-                cot.at[rows], cot_m.at[j - 1, rows], ids["cot"] + j * BLOCKS + b,
-                s, lax.rem(d + 2 * j, N),
-            )
+    parts = ((0, H - H // BLOCKS), (H - H // BLOCKS, H // BLOCKS))
+
+    def strip(side, p):
+        return pl.ds(pl.multiple_of(side * H + parts[p][0], LANES), parts[p][1])
+
+    def send_cot(p):
+        for j in range(1, X):
+            for side in range(2):
+                send(
+                    cot.at[:, strip(side, p)], cot_m.at[j - 1, :, strip(side, p)],
+                    ids["cot"] + (j * 2 + p) * 2 + side, s, lax.rem(d + 2 * j, N),
+                )
+
+    send_cot(0)
     half = pl.ds(pl.multiple_of(c * H, LANES), H)
     ohalf = pl.ds(pl.multiple_of(other * H, LANES), H)
     loads[3].wait()
@@ -465,39 +472,46 @@
     def _():
         ext[:, pl.ds(0, HB), :] = frecv[...].astype(f32)
 
-    def conv_chunk(cb, sums):
+    def convolve(cb, rb):
         tf = kall[cb].astype(f32)
-        parts = []
+        acc = jnp.zeros((RB, LANES), f32)
+        for k in range(K):
+            acc = acc + tf[k : k + 1] * ext[cb, pl.ds(HB - k + rb * RB, RB), :]
+        cen[cb, pl.ds(rb * RB, RB), :] = acc
+        return acc
+
+    def conv_chunk(cb, _):
         for rb in range(T // RB):
-            acc = jnp.zeros((RB, LANES), f32)
-            for k in range(K):
-                acc = acc + tf[k : k + 1] * ext[cb, pl.ds(HB - k + rb * RB, RB), :]
-            cen[cb, pl.ds(rb * RB, RB), :] = acc
-            parts.append(jnp.sum(acc, axis=1, keepdims=True))
-        return sums + jnp.concatenate(parts, axis=0)
-
-    column = jnp.zeros((T, 1), f32)
+            rows = pl.ds(rb * RB, RB)
+            dev = convolve(cb, rb) - means[rows, :]
+            sum1[rows, :] = sum1[rows, :] + dev
+            sum2[rows, :] = sum2[rows, :] + dev * dev
+        return _
+
     with jax.named_scope("conv"):
-        mean = lax.fori_loop(0, chunks, conv_chunk, column) / C
-
-    def square_chunk(cb, sums):
-        dev = cen[cb] - mean
-        return sums + dev * dev
-
-    with jax.named_scope("square"):
-        squares = lax.fori_loop(0, chunks, square_chunk, jnp.zeros((T, LANES), f32))
-    inv = lax.rsqrt(jnp.sum(squares, axis=1, keepdims=True) / C + epsilon)
+        for rb in range(T // RB):
+            rows = pl.ds(rb * RB, RB)
+            acc = convolve(0, rb)
+            start = jnp.broadcast_to(jnp.sum(acc, axis=1, keepdims=True) / LANES, (RB, LANES))
+            means[rows, :] = start
+            sum1[rows, :] = acc - start
+            sum2[rows, :] = (acc - start) * (acc - start)
+        lax.fori_loop(1, chunks, conv_chunk, 0)
+    with jax.named_scope("moments"):
+        shift = jnp.sum(sum1[...], axis=1, keepdims=True) / C
+        variance = jnp.sum(sum2[...], axis=1, keepdims=True) / C - shift * shift
+        means[...] = means[...] + shift
+        invs[...] = jnp.broadcast_to(lax.rsqrt(variance + epsilon), (T, LANES))
 
     def act_chunk(cb, _):
-        centred = (cen[cb] - mean) * inv
+        centred = (cen[cb] - means[...]) * invs[...]
         cen[cb] = centred
         normed = centred * kall[cb].astype(f32)[K : K + 1]
-        act[lax.rem(cb, X), cb // X] = (normed * jax.nn.sigmoid(normed)).astype(bf16)
+        act[lax.rem(cb, X), cb // X] = (normed * jax.nn.sigmoid(normed)).T.astype(bf16)
         return _
 
     with jax.named_scope("act"):
         lax.fori_loop(0, chunks, act_chunk, 0)
-    invs[...] = jnp.broadcast_to(inv, (T, LANES))
     send(act.at[x], act_p.at[0], ids["actp"], s, partner)
 
     near = Z // 2
@@ -518,50 +532,50 @@
                 s, lax.rem(d + 2 * j, N),
             )
 
-    def relay_mirror(b):
-        rows = pl.ds(b * TB, TB)
+    def relay_mirror(p):
+        with jax.named_scope("cotwait%d" % p):
+            for j in range(1, X):
+                for side in range(2):
+                    arrived(cot_m.at[j - 1, :, strip(side, p)], ids["cot"] + (j * 2 + p) * 2 + side)
+                send(
+                    cot_m.at[j - 1, :, strip(other, p)], cot_p.at[j, :, strip(0, p)],
+                    ids["cotp"] + j * 2 + p, s, partner,
+                )
+
+    def project_mirror():
         for j in range(1, X):
-            with jax.named_scope("cotwait%d" % b):
-                arrived(cot_m.at[j - 1, rows], ids["cot"] + j * BLOCKS + b)
-            send(
-                cot_m.at[j - 1, rows, ohalf], cot_p.at[j, rows], ids["cotp"] + j * BLOCKS + b,
-                s, partner,
-            )
-
-    def project_mirror(b):
-        rows = pl.ds(b * TB, TB)
-        for j in range(1, X):
-            with jax.named_scope("proj_m%d" % b):
-                piece = ga_s.at[j - 1, :, rows]
-                project(cot_m.at[j - 1, rows], w, piece, c * cpd)
-                project(cot_m.at[j - 1, rows], w_p, piece, other * cpd)
-            send(
-                piece, ga.at[pl.ds(x * 2 * cpd, 2 * cpd), rows], ids["ga"] + j * BLOCKS + b,
-                s, lax.rem(d + 2 * (X - j), N),
-            )
-
-    dims = (((0,), (0,)), ((), ()))
-    NT = min(H, 512)
-    tiles = H // NT
+            with jax.named_scope("proj_m"):
+                project(cot_m.at[j - 1], w, ga_s.at[j - 1], c * cpd)
+                project(cot_m.at[j - 1], w_p, ga_s.at[j - 1], other * cpd)
+            for b in range(BLOCKS):
+                rows = pl.ds(b * TB, TB)
+                send(
+                    ga_s.at[j - 1, :, rows], ga.at[pl.ds(x * 2 * cpd, 2 * cpd), rows],
+                    ids["ga"] + j * BLOCKS + b, s, lax.rem(d + 2 * (X - j), N),
+                )
+
+    dims = (((1,), (0,)), ((), ()))
 
     def dot(a, b):
         return lax.dot_general(a, b, dims, preferred_element_type=f32)
 
-    def local_part(m, n):
-        cols = pl.ds(pl.multiple_of(n * NT, NT), NT)
-        own = pl.ds(pl.multiple_of(c * H + n * NT, NT), NT)
-        wacc[m, :, cols] = dot(act[x, m], cot[:, own]) + dot(act_p[0, m], cot_p[0, :, cols])
+    LT = H // 2
 
     def local_plane(k):
         def tile(i, _):
-            local_part(plane(k) * Y + i // tiles, lax.rem(i, tiles))
+            m, n = plane(k) * Y + i // 2, lax.rem(i, 2)
+            cols = pl.ds(pl.multiple_of(n * LT, LT), LT)
+            own = pl.ds(pl.multiple_of(c * H + n * LT, LT), LT)
+            wacc[m, :, cols] = dot(act[x, m], cot[:, own]) + dot(act_p[0, m], cot_p[0, :, cols])
             return _
 
         with jax.named_scope("wlocal%d" % k):
             if k == 0:
                 arrived(cot_p.at[0], ids["cotp"])
                 arrived(act_p.at[0], ids["actp"])
-            lax.fori_loop(0, Y * tiles, tile, 0)
+            lax.fori_loop(0, Y * 2, tile, 0)
+
+    NT = H // BLOCKS
 
     def remote_part(m, n):
         cols = pl.ds(pl.multiple_of(n * NT, NT), NT)
@@ -571,17 +585,23 @@
             acc = acc + dot(act_m[j - 1, m], cot_m[j - 1, :, own]) + dot(act_p[j, m], cot_p[j, :, cols])
         return cols, acc
 
-    def weight_plane(k):
+    def relay_act(k):
         piece = pl.ds(plane(k) * Y, Y)
         with jax.named_scope("actwait%d" % k):
             for j in range(1, X):
                 arrived(act_m.at[j - 1, piece], ids["act"] + j * Z + k)
                 send(act_m.at[j - 1, piece], act_p.at[j, piece], ids["actp"] + j * Z + k, s, partner)
+
+    def weight_part(k, p):
+        piece = pl.ds(plane(k) * Y, Y)
+        off, size = parts[p]
+        with jax.named_scope("relaywait%d%d" % (k, p)):
             for j in range(1, X):
-                arrived(act_p.at[j, piece], ids["actp"] + j * Z + k)
-                for b in range(BLOCKS if k == 0 else 0):
-                    arrived(cot_p.at[j, pl.ds(b * TB, TB)], ids["cotp"] + j * BLOCKS + b)
-        with jax.named_scope("wremote%d" % k):
+                if p == 0:
+                    arrived(act_p.at[j, piece], ids["actp"] + j * Z + k)
+                if k == 0:
+                    arrived(cot_p.at[j, :, strip(0, p)], ids["cotp"] + j * 2 + p)
+        with jax.named_scope("wremote%d%d" % (k, p)):
             for j in range(1, Y):
                 to_y = lax.rem(y + j, Y)
                 i = (j - 1) * Z + k
@@ -591,8 +611,11 @@
                     wpart[i, :, cols] = acc.astype(bf16)
                     return _
 
-                lax.fori_loop(0, tiles, send_tile, 0)
-                send(wpart.at[i], yrecv.at[i], ids["y"] + i, z * Y + to_y, d)
+                lax.fori_loop(off // NT, (off + size) // NT, send_tile, 0)
+                send(
+                    wpart.at[i, :, strip(0, p)], yrecv.at[i, :, strip(0, p)],
+                    ids["y"] + i * 2 + p, z * Y + to_y, d,
+                )
 
             def own_tile(n, _):
                 m = plane(k) * Y + y
@@ -600,12 +623,14 @@
                 wacc[m, :, cols] = acc
                 return _
 
-            lax.fori_loop(0, tiles, own_tile, 0)
-
-    def reduce_y(k):
-        with jax.named_scope("ywait%d" % k):
-            for j in range(1, Y):
-                arrived(yrecv.at[(j - 1) * Z + k], ids["y"] + (j - 1) * Z + k)
+            lax.fori_loop(off // NT, (off + size) // NT, own_tile, 0)
+
+    def reduce_y(k, p):
+        for q in (p,) if k < near else (0, 1):
+            with jax.named_scope("ywait%d%d" % (k, q)):
+                for j in range(1, Y):
+                    i = (j - 1) * Z + k
+                    arrived(yrecv.at[i, :, strip(0, q)], ids["y"] + i * 2 + q)
         to_z = plane(k)
         m = to_z * Y + y
 
@@ -620,9 +645,13 @@
                 wacc[m, :, cols] = acc
             return _
 
-        lax.fori_loop(0, H // LANES, tile, 0)
+        off, size = parts[p] if k < near else (0, H)
+        lax.fori_loop(off // LANES, (off + size) // LANES, tile, 0)
         if k < near:
-            r = copy(ysum.at[k], zmid.at[k], ids["z"] + k, inner_z * Y + y, d)
+            r = copy(
+                ysum.at[k, :, strip(0, p)], zmid.at[k, :, strip(0, p)], ids["zmid"] + k * 2 + p,
+                inner_z * Y + y, d,
+            )
 
             @pl.when(jnp.logical_not(inner))
             def _():
@@ -630,25 +659,27 @@
 
             outer.append(r)
         elif k < Z - 1:
-            send(ysum.at[k], zrecv.at[0], ids["z"] + near, to_z * Y + y, d)
-
-    def reduce_z(k):
+            send(ysum.at[k], zrecv.at[0], ids["znear"], to_z * Y + y, d)
+
+    def reduce_z(k, p):
         to_z = plane(k)
         m = to_z * Y + y
+        off, size = parts[p]
 
         def tile(n, _):
             cols = pl.ds(pl.multiple_of(n * LANES, LANES), LANES)
             ysum[k, :, cols] = (wacc[m, :, cols] + zmid[k, :, cols].astype(f32)).astype(bf16)
             return _
 
-        r = copy(ysum.at[k], zrecv.at[1], ids["z"] + k, to_z * Y + y, d, ids["z"] + near + 1)
-
         @pl.when(inner)
         def _():
-            with jax.named_scope("zmid%d" % k):
-                arrived(zmid.at[k], ids["z"] + k)
-            lax.fori_loop(0, H // LANES, tile, 0)
-            r.start()
+            with jax.named_scope("zmid%d%d" % (k, p)):
+                arrived(zmid.at[k, :, strip(0, p)], ids["zmid"] + k * 2 + p)
+            lax.fori_loop(off // LANES, (off + size) // LANES, tile, 0)
+            copy(
+                ysum.at[k, :, strip(0, p)], zrecv.at[1, :, strip(0, p)], ids["zmid"] + k * 2 + p,
+                to_z * Y + y, d, ids["zfar"] + p,
+            ).start()
 
     outer = []
 
@@ -735,28 +766,38 @@
             stores.append(st)
 
     back = copy(bsend, brecv, ids["back"], lax.rem(s + S - 1, S), d)
-    back = copy(bsend, brecv, ids["back"], lax.rem(s + S - 1, S), d)
-    arrived(w_p, ids["w"])
     send_act(0)
     send_act(1)
-    relay_mirror(0)
-    project_mirror(0)
+    send_cot(1)
     send_act(2)
-    relay_mirror(1)
-    project_mirror(1)
     send_act(3)
-    relay_mirror(2)
-    project_mirror(2)
-    local_plane(0)
-    relay_mirror(3)
+    arrived(w_p, ids["w"])
     with jax.named_scope("proj_p"):
         project(cot, w_p, ga, partner * cpd)
-    weight_plane(0)
-    project_mirror(3)
-    for k in (1, 2):
-        local_plane(k)
-        weight_plane(k)
-    reduce_y(0)
+    local_plane(0)
+    local_plane(1)
+    local_plane(2)
+    relay_mirror(0)
+    relay_act(0)
+    weight_part(0, 0)
+    relay_act(1)
+    local_plane(3)
+    weight_part(1, 0)
+    reduce_y(0, 0)
+    relay_mirror(1)
+    project_mirror()
+    weight_part(0, 1)
+    weight_part(1, 1)
+    relay_act(2)
+    reduce_y(1, 0)
+    weight_part(2, 0)
+    weight_part(2, 1)
+    reduce_z(0, 0)
+    reduce_y(0, 1)
+    relay_act(3)
+    reduce_y(1, 1)
+    weight_part(3, 0)
+    weight_part(3, 1)
     gradient(0)
 
     @pl.when(s > 0)
@@ -764,23 +805,41 @@
         back.start()
 
     taps_grad(0)
-    local_plane(3)
-    weight_plane(3)
+    reduce_z(1, 0)
     gradient(1)
     taps_grad(1)
-    reduce_y(1)
+    reduce_z(0, 1)
+    reduce_z(1, 1)
+    reduce_y(2, 0)
     gradient(2)
     taps_grad(2)
-    reduce_z(0)
     gradient(3)
     taps_grad(3)
     for j in range(1, S):
         to = lax.rem(s + j, S)
         send(kgb.at[pl.ds(to * cps, cps)], krecv.at[j], ids["kg"] + j, to, d)
-    reduce_y(2)
+    reduce_y(3, 0)
     gated_grad(0)
-    reduce_z(1)
     gated_grad(1)
+    with jax.named_scope("zwait"):
+        arrived(zrecv.at[0], ids["znear"])
+        for p in range(2):
+            arrived(zrecv.at[1, :, strip(0, p)], ids["zfar"] + p)
+
+    def final_tile(n, _):
+        cols = pl.ds(pl.multiple_of(n * LANES, LANES), LANES)
+        acc = wacc[s, :, cols]
+        for q in range(2):
+            acc = acc + zrecv[q, :, cols].astype(f32)
+        acc = acc * factor
+        fin[0, :, cols] = acc[:block]
+        fin[1, :, cols] = acc[block:]
+        return _
+
+    with jax.named_scope("final"):
+        lax.fori_loop(0, H // LANES, final_tile, 0)
+    send(fin.at[other], fbuf, ids["fin"], s, partner)
+    gw[:, half] = fin[c]
     gated_grad(2)
     with jax.named_scope("backwait"):
         @pl.when(s < S - 1)
@@ -795,7 +854,6 @@
     def _():
         gext[:, pl.ds(T, HB), :] = brecv[...].astype(f32)
 
-    gated_grad(3)
     with jax.named_scope("kgwait"):
         for j in range(1, S):
             arrived(krecv.at[j], ids["kg"] + j)
@@ -805,27 +863,7 @@
     ksum[...] = acc
     for j in range(1, N):
         send(ksum, k2recv.at[j], ids["k2"] + j, s, lax.rem(d + j, N))
-
-    reduce_y(3)
-    with jax.named_scope("zwait"):
-        for q in range(2):
-            arrived(zrecv.at[q], ids["z"] + near + q)
-
-    def final_tile(n, _):
-        cols = pl.ds(pl.multiple_of(n * LANES, LANES), LANES)
-        acc = wacc[s, :, cols]
-        for q in range(2):
-            acc = acc + zrecv[q, :, cols].astype(f32)
-        acc = acc * factor
-        fin[0, :, cols] = acc[:block]
-        fin[1, :, cols] = acc[block:]
-        return _
-
-    with jax.named_scope("final"):
-        lax.fori_loop(0, H // LANES, final_tile, 0)
-    send(fin.at[other], fbuf, ids["fin"], s, partner)
-    gw[:, half] = fin[c]
-
+    gated_grad(3)
     with jax.named_scope("k2wait"):
         for j in range(1, N):
             arrived(k2recv.at[j], ids["k2"] + j)
@@ -884,8 +922,9 @@
     chunks, cps, cpd, block = C // LANES, C // LANES // S, C // LANES // N, C // (S * N)
     M, CR = chunks // X, C // N
     ids, count = number(
-        ("taps", S), ("front", 1), ("back", 1), ("w", 1), ("cot", X * BLOCKS), ("cotp", X * BLOCKS),
-        ("act", X * Z), ("actp", X * Z), ("ga", X * BLOCKS), ("y", (Y - 1) * Z), ("z", Z // 2 + 2), ("fin", 1),
+        ("taps", S), ("front", 1), ("back", 1), ("w", 1), ("cot", X * 4), ("cotp", X * 2),
+        ("act", X * Z), ("actp", X * Z), ("ga", X * BLOCKS), ("y", (Y - 1) * Z * 2), ("zmid", Z), ("znear", 1), ("zfar", 2),
+        ("fin", 1),
         ("kg", S), ("k2", N),
     )
     vm = pl.BlockSpec(memory_space=pltpu.VMEM)
@@ -918,9 +957,9 @@
             pltpu.VMEM((chunks, T, LANES), f32),
             pltpu.VMEM((chunks, T + HB, LANES), f32),
             pltpu.VMEM((chunks, KP, LANES), bf16),
-            pltpu.VMEM((X, M, T, LANES), bf16),
-            pltpu.VMEM((X - 1, M, T, LANES), bf16),
-            pltpu.VMEM((X, M, T, LANES), bf16),
+            pltpu.VMEM((X, M, LANES, T), bf16),
+            pltpu.VMEM((X - 1, M, LANES, T), bf16),
+            pltpu.VMEM((X, M, LANES, T), bf16),
             pltpu.VMEM((X - 1, 2 * cpd, T, LANES), bf16),
             pltpu.VMEM((chunks, T, LANES), bf16),
             pltpu.VMEM((M, LANES, H), f32),
@@ -933,6 +972,9 @@
             pltpu.VMEM((block, H), f32),
             pltpu.VMEM((T, C), bf16),
             pltpu.VMEM((T, C), bf16),
+            pltpu.VMEM((T, LANES), f32),
+            pltpu.VMEM((T, LANES), f32),
+            pltpu.VMEM((T, LANES), f32),
             pltpu.VMEM((T, LANES), f32),
             pltpu.VMEM((chunks, K + 1, 8, LANES), f32),
             pltpu.VMEM((chunks, KP, LANES), f32),

time: 78.7 us -> 73 us (0.928)
  Pallas kernels: 77.7 us -> 72.1 us
    pallas_call x1, Pallas kernels: 73.8 us -> 68.1 us  [pair_call(): pl.pallas_call(functools.partial(pair_kernel, S, N, Y, T, C, K, HB, ids),...]
where the time goes in v3:
time: 73 us; the launch traced here: 72.7 us
  Pallas kernels  72.1 us (99%)
    pallas_call x1, Pallas kernels, pair_call(): pl.pallas_call(functools.partial(pair_kernel, S, N, Y, T, C, K, HB, ids),...  68.1 us
    pallas_call x1, Pallas kernels, pair_call(): pl.pallas_call(functools.partial(hand_over, K), out_shape=(jax.ShapeDtype...  3.99 us

profile of v3, /device:TPU:0, one launch (start us, length us, event | category | flops | bytes accessed | tf_op | source)
XLA Modules:
  0.0 72.7 jit_solution(2372926220293627356)
XLA Ops:
  0.6 68.1 %block_backward.1 = (bf16[256,2048]{1,0:T(8,128)(2,1)}, bf16[256,2048]{1,0:T(8,128)(2,1)}, f32[64,2048]{1,0:T(8,128)}, f32[32,256]{1,0:T(8,128)}) custom-call(bf16[256,2048]{1,0:T(8,128)(2,1)} %bitcast.6, bf16[256,2048]{1,0:T(8,128)(2,1)} %bitcast.7, bf16[256,2048]{1,0:T(8,128)(2,1)} %bitcast.8, bf16[512,2048]{1,0:T(8,128)(2,1)} %w_in.1, ...), custom_call_target="tpu_custom_call" | custom-call | tf_op jit(solution)/shard_map/block_backward/pallas_call | solution.py:932
  68.7 4.0 %hand_over.1 = (bf16[256,2048]{1,0:T(8,128)(2,1)}, bf16[256,2048]{1,0:T(8,128)(2,1)}, f32[64,2048]{1,0:T(8,128)}, f32[31,256]{1,0:T(8,128)}, f32[1,256]{1,0:T(1,128)}) custom-call(bf16[256,2048]{1,0:T(8,128)(2,1)} %get-tuple-element.14.gv_in, bf16[256,2048]{1,0:T(8,128)(2,1)} %get-tuple-element.15.gg_in, f32[64,2048]{1,0:T(8,128)} %get-tuple-element.16.gw_in, ...), custom_call_target="tpu_custom_call" | custom-call | tf_op jit(solution)/shard_map/hand_over/pallas_call | solution.py:996

commit v4 on v3

--- a/solution.py
+++ b/solution.py
@@ -314,11 +314,11 @@
 
 def pair_kernel(
     S, N, Y, T, C, K, HB, ids,
-    cot_in, val_in, gate_in, w_in, kernel, gain,
-    gv_out, gg_out, gw, kout,
-    taps, cot, val, gate, w, w_p, cot_m, cot_p, fsend, frecv, bsend, brecv, ext, cen, gc, gext, kall,
-    act, act_m, act_p, ga_s, ga, wacc, wpart, yrecv, ysum, zmid, zrecv, fin, fbuf, gv, gg,
-    means, invs, sum1, sum2, kacc, kg, kgb, krecv, ksum, k2recv, send_sem, recv_sem, load_sem, store_sem, ready,
+    cot_in, val_in, gate_in, w_in, kernel_in, gain_in,
+    gv, gg, gw, kout,
+    kernel, gain, taps, cot, val, gate, w, w_p, cot_m, cot_p, fsend, frecv, bsend, brecv, ext, cen, gc, gext, kall,
+    act, act_m, act_p, ga_s, ga, wacc, wpart, yrecv, ysum, zmid, zrecv, fin, fbuf,
+    means, invs, sum1, sum2, kacc, kg, kgb, krecv, ksum, k2recv, send_sem, recv_sem, load_sem, ready,
 ):
     s = lax.axis_index("sp")
     d = lax.axis_index("dp")
@@ -354,7 +354,9 @@
 
     loads = [
         pltpu.make_async_copy(a, b, load_sem.at[i])
-        for i, (a, b) in enumerate(((gate_in, gate), (val_in, val), (cot_in, cot), (w_in, w)))
+        for i, (a, b) in enumerate((
+            (gate_in, gate), (val_in, val), (cot_in, cot), (w_in, w), (kernel_in, kernel), (gain_in, gain),
+        ))
     ]
     for l in loads:
         l.start()
@@ -381,6 +383,46 @@
     for j in range(1, Y):
         signal(barrier, z * Y + lax.rem(y + j, Y), d)
     along_z(lambda side, to_s: signal(barrier, to_s, d))
+    loads[2].wait()
+    with jax.named_scope("barrierwait"):
+        pl.semaphore_wait(barrier, X + Y - 1 + jnp.where(z > 0, 1, 0) + jnp.where(z < Z - 1, 1, 0))
+
+    def pass_on(r):
+        along_z(lambda side, to_s: signal(ready.at[2 * r + 1 - side], to_s, d))
+
+    def passed(r):
+        along_z(lambda side, to_s: pl.semaphore_wait(ready.at[2 * r + side], 1))
+
+    pass_on(0)
+    parts = ((0, H - H // BLOCKS), (H - H // BLOCKS, H // BLOCKS))
+
+    def strip(side, p):
+        return pl.ds(pl.multiple_of(side * H + parts[p][0], LANES), parts[p][1])
+
+    def send_cot(p):
+        for j in range(1, X):
+            for side in range(2):
+                send(
+                    cot.at[:, strip(side, p)], cot_m.at[j - 1, :, strip(side, p)],
+                    ids["cot"] + (j * 2 + p) * 2 + side, s, lax.rem(d + 2 * j, N),
+                )
+
+    send_cot(0)
+    loads[0].wait()
+    loads[1].wait()
+
+    def gate_chunk(cb, _):
+        cols = pl.ds(pl.multiple_of(cb * LANES, LANES), LANES)
+        sig = jax.nn.sigmoid(gate[:, cols].astype(f32))
+        gated = (val[:, cols].astype(f32) * sig).astype(bf16)
+        ext[cb, pl.ds(HB, T), :] = gated.astype(f32)
+        fsend[cb] = gated[T - HB :]
+        return _
+
+    with jax.named_scope("gate"):
+        lax.fori_loop(0, chunks, gate_chunk, 0)
+    loads[4].wait()
+    loads[5].wait()
     KP = taps.shape[1]
     for q in range(cps):
         cols = slice(q * LANES, (q + 1) * LANES)
@@ -389,37 +431,6 @@
             + [jnp.zeros((KP - K - 1, LANES), f32)] * (KP > K + 1),
             axis=0,
         ).astype(bf16)
-    loads[0].wait()
-    loads[1].wait()
-
-    def gate_chunk(cb, _):
-        cols = pl.ds(pl.multiple_of(cb * LANES, LANES), LANES)
-        sig = jax.nn.sigmoid(gate[:, cols].astype(f32))
-        gated = (val[:, cols].astype(f32) * sig).astype(bf16)
-        ext[cb, pl.ds(HB, T), :] = gated.astype(f32)
-        fsend[cb] = gated[T - HB :]
-        return _
-
-    with jax.named_scope("gate"):
-        lax.fori_loop(0, chunks, gate_chunk, 0)
-    loads[2].wait()
-    with jax.named_scope("barrierwait"):
-        pl.semaphore_wait(barrier, X + Y - 1 + jnp.where(z > 0, 1, 0) + jnp.where(z < Z - 1, 1, 0))
-
-    parts = ((0, H - H // BLOCKS), (H - H // BLOCKS, H // BLOCKS))
-
-    def strip(side, p):
-        return pl.ds(pl.multiple_of(side * H + parts[p][0], LANES), parts[p][1])
-
-    def send_cot(p):
-        for j in range(1, X):
-            for side in range(2):
-                send(
-                    cot.at[:, strip(side, p)], cot_m.at[j - 1, :, strip(side, p)],
-                    ids["cot"] + (j * 2 + p) * 2 + side, s, lax.rem(d + 2 * j, N),
-                )
-
-    send_cot(0)
     half = pl.ds(pl.multiple_of(c * H, LANES), H)
     ohalf = pl.ds(pl.multiple_of(other * H, LANES), H)
     loads[3].wait()
@@ -428,8 +439,9 @@
     kall[pl.ds(s * cps, cps)] = taps[...]
     with jax.named_scope("ready"):
         for r in range(Z - 2):
-            along_z(lambda side, to_s: signal(ready.at[2 * r + 1 - side], to_s, d))
-            along_z(lambda side, to_s: pl.semaphore_wait(ready.at[2 * r + side], 1))
+            if r > 0:
+                pass_on(r)
+            passed(r)
         for j in range(1, Y):
             signal(ready.at[2 * (Z - 2)], z * Y + lax.rem(y + j, Y), d)
         pl.semaphore_wait(ready.at[2 * (Z - 2)], Y - 1)
@@ -524,13 +536,19 @@
             return jnp.where(low, Z - 1 - k, k)
         return jnp.where(low, 0, near) + lax.rem(z + 1 + k, near)
 
-    def send_act(k):
-        piece = pl.ds(plane(k) * Y, Y)
-        for j in range(1, X):
-            send(
-                act.at[lax.rem(x + j, X), piece], act_m.at[j - 1, piece], ids["act"] + j * Z + k,
-                s, lax.rem(d + 2 * j, N),
-            )
+    def planes(k, own):
+        if k < Z - 1:
+            return [(plane(k) * Y, Y, 0)]
+        return [(plane(k) * Y + lax.rem(y + j, Y), 1, j) for j in (range(1) if own else range(1, Y))]
+
+    def send_act(k, own=False):
+        for first, size, n in planes(k, own):
+            piece = pl.ds(first, size)
+            for j in range(1, X):
+                send(
+                    act.at[lax.rem(x + j, X), piece], act_m.at[j - 1, piece],
+                    ids["act"] + (j * Z + k) * Y + n, s, lax.rem(d + 2 * j, N),
+                )
 
     def relay_mirror(p):
         with jax.named_scope("cotwait%d" % p):
@@ -585,22 +603,37 @@
             acc = acc + dot(act_m[j - 1, m], cot_m[j - 1, :, own]) + dot(act_p[j, m], cot_p[j, :, cols])
         return cols, acc
 
-    def relay_act(k):
-        piece = pl.ds(plane(k) * Y, Y)
+    def relay_act(k, own=False):
         with jax.named_scope("actwait%d" % k):
+            for first, size, n in planes(k, own):
+                piece = pl.ds(first, size)
+                for j in range(1, X):
+                    i = (j * Z + k) * Y + n
+                    arrived(act_m.at[j - 1, piece], ids["act"] + i)
+                    send(act_m.at[j - 1, piece], act_p.at[j, piece], ids["actp"] + i, s, partner)
+
+    def relayed(k, own=False):
+        with jax.named_scope("relaywait%d" % k):
+            for first, size, n in planes(k, own):
+                for j in range(1, X):
+                    arrived(act_p.at[j, pl.ds(first, size)], ids["actp"] + (j * Z + k) * Y + n)
+
+    def own_part(k, off, size):
+        def own_tile(n, _):
+            m = plane(k) * Y + y
+            cols, acc = remote_part(m, n)
+            wacc[m, :, cols] = acc
+            return _
+
+        lax.fori_loop(off // NT, (off + size) // NT, own_tile, 0)
+
+    def weight_part(k, p):
+        off, size = parts[p]
+        if p == 0:
+            relayed(k)
+        if k == 0:
             for j in range(1, X):
-                arrived(act_m.at[j - 1, piece], ids["act"] + j * Z + k)
-                send(act_m.at[j - 1, piece], act_p.at[j, piece], ids["actp"] + j * Z + k, s, partner)
-
-    def weight_part(k, p):
-        piece = pl.ds(plane(k) * Y, Y)
-        off, size = parts[p]
-        with jax.named_scope("relaywait%d%d" % (k, p)):
-            for j in range(1, X):
-                if p == 0:
-                    arrived(act_p.at[j, piece], ids["actp"] + j * Z + k)
-                if k == 0:
-                    arrived(cot_p.at[j, :, strip(0, p)], ids["cotp"] + j * 2 + p)
+                arrived(cot_p.at[j, :, strip(0, p)], ids["cotp"] + j * 2 + p)
         with jax.named_scope("wremote%d%d" % (k, p)):
             for j in range(1, Y):
                 to_y = lax.rem(y + j, Y)
@@ -617,16 +650,11 @@
                     ids["y"] + i * 2 + p, z * Y + to_y, d,
                 )
 
-            def own_tile(n, _):
-                m = plane(k) * Y + y
-                cols, acc = remote_part(m, n)
-                wacc[m, :, cols] = acc
-                return _
-
-            lax.fori_loop(off // NT, (off + size) // NT, own_tile, 0)
+            if k < Z - 1:
+                own_part(k, off, size)
 
     def reduce_y(k, p):
-        for q in (p,) if k < near else (0, 1):
+        for q in (p,) if k < Z - 1 else (0, 1):
             with jax.named_scope("ywait%d%d" % (k, q)):
                 for j in range(1, Y):
                     i = (j - 1) * Z + k
@@ -645,7 +673,7 @@
                 wacc[m, :, cols] = acc
             return _
 
-        off, size = parts[p] if k < near else (0, H)
+        off, size = parts[p] if k < Z - 1 else (0, H)
         lax.fori_loop(off // LANES, (off + size) // LANES, tile, 0)
         if k < near:
             r = copy(
@@ -659,7 +687,10 @@
 
             outer.append(r)
         elif k < Z - 1:
-            send(ysum.at[k], zrecv.at[0], ids["znear"], to_z * Y + y, d)
+            send(
+                ysum.at[k, :, strip(0, p)], zrecv.at[0, :, strip(0, p)], ids["znear"] + p,
+                to_z * Y + y, d,
+            )
 
     def reduce_z(k, p):
         to_z = plane(k)
@@ -741,8 +772,6 @@
         with jax.named_scope("taps%d" % b):
             lax.fori_loop(0, chunks, taps_chunk, 0)
 
-    stores = []
-
     def gated_grad(b):
         rows = pl.ds(b * TB, TB)
 
@@ -760,10 +789,6 @@
 
         with jax.named_scope("gated%d" % b):
             lax.fori_loop(0, chunks, gated_chunk, 0)
-        for i, (src, dst) in enumerate(((gv, gv_out), (gg, gg_out))):
-            st = pltpu.make_async_copy(src.at[rows], dst.at[rows], store_sem.at[2 * b + i])
-            st.start()
-            stores.append(st)
 
     back = copy(bsend, brecv, ids["back"], lax.rem(s + S - 1, S), d)
     send_act(0)
@@ -783,18 +808,19 @@
     relay_act(1)
     local_plane(3)
     weight_part(1, 0)
-    reduce_y(0, 0)
     relay_mirror(1)
     project_mirror()
+    send_act(Z - 1, own=True)
+    reduce_y(0, 0)
     weight_part(0, 1)
     weight_part(1, 1)
     relay_act(2)
-    reduce_y(1, 0)
+    relay_act(3)
     weight_part(2, 0)
     weight_part(2, 1)
+    reduce_y(1, 0)
     reduce_z(0, 0)
     reduce_y(0, 1)
-    relay_act(3)
     reduce_y(1, 1)
     weight_part(3, 0)
     weight_part(3, 1)
@@ -805,25 +831,44 @@
         back.start()
 
     taps_grad(0)
-    reduce_z(1, 0)
     gradient(1)
     taps_grad(1)
+    reduce_z(1, 0)
+    gradient(2)
+    taps_grad(2)
+    reduce_y(2, 0)
     reduce_z(0, 1)
     reduce_z(1, 1)
-    reduce_y(2, 0)
-    gradient(2)
-    taps_grad(2)
     gradient(3)
     taps_grad(3)
     for j in range(1, S):
         to = lax.rem(s + j, S)
         send(kgb.at[pl.ds(to * cps, cps)], krecv.at[j], ids["kg"] + j, to, d)
+    reduce_y(2, 1)
+    relay_act(3, own=True)
+    gated_grad(0)
+    relayed(3, own=True)
+    own_part(3, 0, H)
     reduce_y(3, 0)
-    gated_grad(0)
     gated_grad(1)
+    gated_grad(2)
+    with jax.named_scope("drain"):
+        for r in waits + outer:
+            r.wait_send()
+        waits.clear()
+        outer.clear()
+    with jax.named_scope("kgwait"):
+        for j in range(1, S):
+            arrived(krecv.at[j], ids["kg"] + j)
+    acc = kg[pl.ds(s * cps, cps)]
+    for j in range(1, S):
+        acc = acc + krecv[j].astype(f32)
+    ksum[...] = acc
+    for j in range(1, N):
+        send(ksum, k2recv.at[j], ids["k2"] + j, s, lax.rem(d + j, N))
     with jax.named_scope("zwait"):
-        arrived(zrecv.at[0], ids["znear"])
         for p in range(2):
+            arrived(zrecv.at[0, :, strip(0, p)], ids["znear"] + p)
             arrived(zrecv.at[1, :, strip(0, p)], ids["zfar"] + p)
 
     def final_tile(n, _):
@@ -840,7 +885,6 @@
         lax.fori_loop(0, H // LANES, final_tile, 0)
     send(fin.at[other], fbuf, ids["fin"], s, partner)
     gw[:, half] = fin[c]
-    gated_grad(2)
     with jax.named_scope("backwait"):
         @pl.when(s < S - 1)
         def _():
@@ -854,15 +898,6 @@
     def _():
         gext[:, pl.ds(T, HB), :] = brecv[...].astype(f32)
 
-    with jax.named_scope("kgwait"):
-        for j in range(1, S):
-            arrived(krecv.at[j], ids["kg"] + j)
-    acc = kg[pl.ds(s * cps, cps)]
-    for j in range(1, S):
-        acc = acc + krecv[j].astype(f32)
-    ksum[...] = acc
-    for j in range(1, N):
-        send(ksum, k2recv.at[j], ids["k2"] + j, s, lax.rem(d + j, N))
     gated_grad(3)
     with jax.named_scope("k2wait"):
         for j in range(1, N):
@@ -874,7 +909,7 @@
 
     arrived(fbuf, ids["fin"])
     gw[:, ohalf] = fbuf[...]
-    for r in waits + outer:
+    for r in waits:
         r.wait_send()
 
     @pl.when(s < S - 1)
@@ -884,9 +919,6 @@
     @pl.when(s > 0)
     def _():
         back.wait_send()
-
-    for st in stores:
-        st.wait()
 
 
 def number(*sizes):
@@ -897,22 +929,13 @@
     return ids, count
 
 
-def hand_over(K, gv_in, gg_in, gw_in, k_in, gv, gg, gw, kout, gout, a, b, c, sem):
-    T = gv_in.shape[0]
-    pieces = []
-    for n in range(2):
-        rows = pl.ds(n * (T // 2), T // 2)
-        pieces += [(gv_in.at[rows], a.at[rows], gv.at[rows]), (gg_in.at[rows], b.at[rows], gg.at[rows])]
-    pieces.append((gw_in, c, gw))
-    loads = [pltpu.make_async_copy(p[0], p[1], sem.at[0, i]) for i, p in enumerate(pieces)]
-    stores = [pltpu.make_async_copy(p[1], p[2], sem.at[1, i]) for i, p in enumerate(pieces)]
-    for l in loads:
-        l.start()
+def hand_over(K, gv_in, gg_in, gw_in, k_in, gv, gg, gw, kout, gout, sem):
+    pieces = ((gv_in, gv), (gg_in, gg), (gw_in, gw))
+    stores = [pltpu.make_async_copy(a, b, sem.at[i]) for i, (a, b) in enumerate(pieces)]
+    for st in stores:
+        st.start()
     kout[...] = k_in[:K]
     gout[...] = k_in[K : K + 1]
-    for l, st in zip(loads, stores):
-        l.wait()
-        st.start()
     for st in stores:
         st.wait()
 
@@ -923,7 +946,7 @@
     M, CR = chunks // X, C // N
     ids, count = number(
         ("taps", S), ("front", 1), ("back", 1), ("w", 1), ("cot", X * 4), ("cotp", X * 2),
-        ("act", X * Z), ("actp", X * Z), ("ga", X * BLOCKS), ("y", (Y - 1) * Z * 2), ("zmid", Z), ("znear", 1), ("zfar", 2),
+        ("act", X * Z * Y), ("actp", X * Z * Y), ("ga", X * BLOCKS), ("y", (Y - 1) * Z * 2), ("zmid", Z), ("znear", 2), ("zfar", 2),
         ("fin", 1),
         ("kg", S), ("k2", N),
     )
@@ -937,9 +960,11 @@
             jax.ShapeDtypeStruct((block, C), f32),
             jax.ShapeDtypeStruct((KP, C // S), f32),
         ),
-        in_specs=[hbm] * 4 + [vm] * 2,
-        out_specs=(hbm, hbm, vm, vm),
+        in_specs=[hbm] * 6,
+        out_specs=(vm,) * 4,
         scratch_shapes=[
+            pltpu.VMEM((K, C // S), bf16),
+            pltpu.VMEM((C // S,), bf16),
             pltpu.VMEM((cps, KP, LANES), bf16),
             pltpu.VMEM((T, C), bf16),
             pltpu.VMEM((T, C), bf16),
@@ -970,8 +995,6 @@
             pltpu.VMEM((2, LANES, H), bf16),
             pltpu.VMEM((2, block, H), f32),
             pltpu.VMEM((block, H), f32),
-            pltpu.VMEM((T, C), bf16),
-            pltpu.VMEM((T, C), bf16),
             pltpu.VMEM((T, LANES), f32),
             pltpu.VMEM((T, LANES), f32),
             pltpu.VMEM((T, LANES), f32),
@@ -984,15 +1007,14 @@
             pltpu.VMEM((N, cps, KP, LANES), f32),
             pltpu.SemaphoreType.DMA((count,)),
             pltpu.SemaphoreType.DMA((count,)),
-            pltpu.SemaphoreType.DMA((4,)),
-            pltpu.SemaphoreType.DMA((2 * BLOCKS,)),
+            pltpu.SemaphoreType.DMA((6,)),
             pltpu.SemaphoreType.REGULAR((2 * (Z - 2) + 1,)),
         ],
         compiler_params=pltpu.CompilerParams(
-            collective_id=0, has_side_effects=True, vmem_limit_bytes=62 * 1024 * 1024
+            collective_id=0, has_side_effects=True, vmem_limit_bytes=48 * 1024 * 1024
         ),
         name="block_backward",
-    )(cot, val, gate, w, kernel, gain)
+    )(*(pltpu.with_memory_space_constraint(a, pltpu.HBM) for a in (cot, val, gate, w, kernel, gain)))
     return pl.pallas_call(
         functools.partial(hand_over, K),
         out_shape=(
@@ -1002,14 +1024,12 @@
             jax.ShapeDtypeStruct((K, C // S), f32),
             jax.ShapeDtypeStruct((1, C // S), f32),
         ),
-        in_specs=[hbm] * 3 + [vm],
+        in_specs=[vm] * 4,
         out_specs=(hbm, hbm, hbm, vm, vm),
         scratch_shapes=[
-            pltpu.VMEM((T, C), bf16),
-            pltpu.VMEM((T, C), bf16),
-            pltpu.VMEM((block, C), f32),
-            pltpu.SemaphoreType.DMA((2, 5)),
+            pltpu.SemaphoreType.DMA((3,)),
         ],
+        compiler_params=pltpu.CompilerParams(vmem_limit_bytes=16 * T * LANES),
         name="hand_over",
     )(*partial)
 

time: 73 us -> 69.4 us (0.951)
  Pallas kernels: 72.1 us -> 68.6 us
    pallas_call x1, Pallas kernels: 3.99 us -> 2.13 us  [pair_call(): pl.pallas_call(functools.partial(hand_over, K), out_shape=(jax.ShapeDtype...]
    pallas_call x1, Pallas kernels: 68.1 us -> 66.4 us  [pair_call(): pl.pallas_call(functools.partial(pair_kernel, S, N, Y, T, C, K, HB, ids),...]
where the time goes in v4:
time: 69.4 us; the launch traced here: 69.2 us
  Pallas kernels  68.6 us (99%)
    pallas_call x1, Pallas kernels, pair_call(): pl.pallas_call(functools.partial(pair_kernel, S, N, Y, T, C, K, HB, ids),...  66.4 us
    pallas_call x1, Pallas kernels, pair_call(): pl.pallas_call(functools.partial(hand_over, K), out_shape=(jax.ShapeDtype...  2.13 us

profile of v4, /device:TPU:0, one launch (start us, length us, event | category | flops | bytes accessed | tf_op | source)
XLA Modules:
  0.0 69.2 jit_solution(11718977761455657068)
XLA Ops:
  0.6 66.4 %block_backward.1 = (bf16[256,2048]{1,0:T(8,128)(2,1)S(1)}, bf16[256,2048]{1,0:T(8,128)(2,1)S(1)}, f32[64,2048]{1,0:T(8,128)S(1)}, f32[32,256]{1,0:T(8,128)S(1)}) custom-call(bf16[256,2048]{1,0:T(8,128)(2,1)} %bitcast.6, bf16[256,2048]{1,0:T(8,128)(2,1)} %bitcast.7, bf16[256,2048]{1,0:T(8,128)(2,1)} %bitcast.8, bf16[512,2048]{1,0:T(8,128)(2,1)} %w_in.1, ...), custom_call_target="tpu_custom_call" | custom-call | tf_op jit(solution)/shard_map/block_backward/pallas_call | solution.py:955
  67.1 2.1 %hand_over.1 = (bf16[256,2048]{1,0:T(8,128)(2,1)}, bf16[256,2048]{1,0:T(8,128)(2,1)}, f32[64,2048]{1,0:T(8,128)}, f32[31,256]{1,0:T(8,128)}, f32[1,256]{1,0:T(1,128)}) custom-call(bf16[256,2048]{1,0:T(8,128)(2,1)S(1)} %get-tuple-element.14.gv_in, bf16[256,2048]{1,0:T(8,128)(2,1)S(1)} %get-tuple-element.15.gg_in, f32[64,2048]{1,0:T(8,128)S(1)} %get-tuple-element.16.gw_in, ...), custom_call_target="tpu_custom_call" | custom-call | tf_op jit(solution)/shard_map/hand_over/pallas_call | solution.py:1018

commit v5 on v4

--- a/solution.py
+++ b/solution.py
@@ -394,10 +394,15 @@
         along_z(lambda side, to_s: pl.semaphore_wait(ready.at[2 * r + side], 1))
 
     pass_on(0)
-    parts = ((0, H - H // BLOCKS), (H - H // BLOCKS, H // BLOCKS))
+    strips = ((0, H - H // BLOCKS), (H - H // BLOCKS, H // BLOCKS))
+    parts = ((0, H // 2), (H // 2, H // BLOCKS), (H - H // BLOCKS, H // BLOCKS))
+    P = len(parts)
 
     def strip(side, p):
-        return pl.ds(pl.multiple_of(side * H + parts[p][0], LANES), parts[p][1])
+        return pl.ds(pl.multiple_of(side * H + strips[p][0], LANES), strips[p][1])
+
+    def part(p):
+        return pl.ds(parts[p][0], parts[p][1])
 
     def send_cot(p):
         for j in range(1, X):
@@ -631,9 +636,10 @@
         off, size = parts[p]
         if p == 0:
             relayed(k)
-        if k == 0:
+        if k == 0 and p != 1:
+            q = 0 if p == 0 else 1
             for j in range(1, X):
-                arrived(cot_p.at[j, :, strip(0, p)], ids["cotp"] + j * 2 + p)
+                arrived(cot_p.at[j, :, strip(0, q)], ids["cotp"] + j * 2 + q)
         with jax.named_scope("wremote%d%d" % (k, p)):
             for j in range(1, Y):
                 to_y = lax.rem(y + j, Y)
@@ -646,19 +652,19 @@
 
                 lax.fori_loop(off // NT, (off + size) // NT, send_tile, 0)
                 send(
-                    wpart.at[i, :, strip(0, p)], yrecv.at[i, :, strip(0, p)],
-                    ids["y"] + i * 2 + p, z * Y + to_y, d,
+                    wpart.at[i, :, part(p)], yrecv.at[i, :, part(p)],
+                    ids["y"] + i * P + p, z * Y + to_y, d,
                 )
 
             if k < Z - 1:
                 own_part(k, off, size)
 
     def reduce_y(k, p):
-        for q in (p,) if k < Z - 1 else (0, 1):
+        for q in (p,) if k < Z - 1 else range(P):
             with jax.named_scope("ywait%d%d" % (k, q)):
                 for j in range(1, Y):
                     i = (j - 1) * Z + k
-                    arrived(yrecv.at[i, :, strip(0, q)], ids["y"] + i * 2 + q)
+                    arrived(yrecv.at[i, :, part(q)], ids["y"] + i * P + q)
         to_z = plane(k)
         m = to_z * Y + y
 
@@ -677,7 +683,7 @@
         lax.fori_loop(off // LANES, (off + size) // LANES, tile, 0)
         if k < near:
             r = copy(
-                ysum.at[k, :, strip(0, p)], zmid.at[k, :, strip(0, p)], ids["zmid"] + k * 2 + p,
+                ysum.at[k, :, part(p)], zmid.at[k, :, part(p)], ids["zmid"] + k * P + p,
                 inner_z * Y + y, d,
             )
 
@@ -688,7 +694,7 @@
             outer.append(r)
         elif k < Z - 1:
             send(
-                ysum.at[k, :, strip(0, p)], zrecv.at[0, :, strip(0, p)], ids["znear"] + p,
+                ysum.at[k, :, part(p)], zrecv.at[0, :, part(p)], ids["znear"] + p,
                 to_z * Y + y, d,
             )
 
@@ -705,10 +711,10 @@
         @pl.when(inner)
         def _():
             with jax.named_scope("zmid%d%d" % (k, p)):
-                arrived(zmid.at[k, :, strip(0, p)], ids["zmid"] + k * 2 + p)
+                arrived(zmid.at[k, :, part(p)], ids["zmid"] + k * P + p)
             lax.fori_loop(off // LANES, (off + size) // LANES, tile, 0)
             copy(
-                ysum.at[k, :, strip(0, p)], zrecv.at[1, :, strip(0, p)], ids["zmid"] + k * 2 + p,
+                ysum.at[k, :, part(p)], zrecv.at[1, :, part(p)], ids["zmid"] + k * P + p,
                 to_z * Y + y, d, ids["zfar"] + p,
             ).start()
 
@@ -752,6 +758,10 @@
 
         with jax.named_scope("convgrad%d" % b):
             lax.fori_loop(0, chunks, conv_grad, 0)
+
+    def kg_copy(off):
+        to = lax.rem(s + off, S)
+        return copy(kgb.at[pl.ds(to * cps, cps)], krecv.at[off], ids["kg"] + off, to, d)
 
     def taps_grad(b):
         def taps_chunk(cb, _):
@@ -769,8 +779,19 @@
                 kgb[cb] = kg[cb].astype(bf16)
             return _
 
+        def taps_owner(n, _):
+            off = 1 + lax.rem(n + S // 2 - 1, S - 1)
+            to = lax.rem(s + off, S)
+            lax.fori_loop(to * cps, to * cps + cps, taps_chunk, 0)
+            kg_copy(off).start()
+            return _
+
         with jax.named_scope("taps%d" % b):
-            lax.fori_loop(0, chunks, taps_chunk, 0)
+            if b < BLOCKS - 1:
+                lax.fori_loop(0, chunks, taps_chunk, 0)
+            else:
+                lax.fori_loop(0, S - 1, taps_owner, 0)
+                lax.fori_loop(s * cps, s * cps + cps, taps_chunk, 0)
 
     def gated_grad(b):
         rows = pl.ds(b * TB, TB)
@@ -805,25 +826,31 @@
     relay_mirror(0)
     relay_act(0)
     weight_part(0, 0)
+    weight_part(0, 1)
     relay_act(1)
     local_plane(3)
     weight_part(1, 0)
+    weight_part(1, 1)
     relay_mirror(1)
+    reduce_y(0, 0)
     project_mirror()
-    send_act(Z - 1, own=True)
-    reduce_y(0, 0)
-    weight_part(0, 1)
-    weight_part(1, 1)
+    send_act(3, own=True)
+    reduce_y(0, 1)
+    weight_part(0, 2)
+    weight_part(1, 2)
     relay_act(2)
-    relay_act(3)
-    weight_part(2, 0)
-    weight_part(2, 1)
     reduce_y(1, 0)
     reduce_z(0, 0)
-    reduce_y(0, 1)
+    relay_act(3)
     reduce_y(1, 1)
-    weight_part(3, 0)
-    weight_part(3, 1)
+    for p in range(P):
+        weight_part(2, p)
+    reduce_z(0, 1)
+    reduce_y(0, 2)
+    reduce_y(1, 2)
+    for p in range(P):
+        weight_part(3, p)
+    reduce_z(1, 0)
     gradient(0)
 
     @pl.when(s > 0)
@@ -831,26 +858,25 @@
         back.start()
 
     taps_grad(0)
+    reduce_z(1, 1)
     gradient(1)
     taps_grad(1)
-    reduce_z(1, 0)
+    reduce_z(0, 2)
+    reduce_z(1, 2)
     gradient(2)
     taps_grad(2)
     reduce_y(2, 0)
-    reduce_z(0, 1)
-    reduce_z(1, 1)
+    reduce_y(2, 1)
     gradient(3)
     taps_grad(3)
-    for j in range(1, S):
-        to = lax.rem(s + j, S)
-        send(kgb.at[pl.ds(to * cps, cps)], krecv.at[j], ids["kg"] + j, to, d)
-    reduce_y(2, 1)
+    waits.extend(kg_copy(j) for j in range(1, S))
+    reduce_y(2, 2)
     relay_act(3, own=True)
     gated_grad(0)
+    gated_grad(1)
     relayed(3, own=True)
     own_part(3, 0, H)
     reduce_y(3, 0)
-    gated_grad(1)
     gated_grad(2)
     with jax.named_scope("drain"):
         for r in waits + outer:
@@ -867,9 +893,9 @@
     for j in range(1, N):
         send(ksum, k2recv.at[j], ids["k2"] + j, s, lax.rem(d + j, N))
     with jax.named_scope("zwait"):
-        for p in range(2):
-            arrived(zrecv.at[0, :, strip(0, p)], ids["znear"] + p)
-            arrived(zrecv.at[1, :, strip(0, p)], ids["zfar"] + p)
+        for p in range(P):
+            arrived(zrecv.at[0, :, part(p)], ids["znear"] + p)
+            arrived(zrecv.at[1, :, part(p)], ids["zfar"] + p)
 
     def final_tile(n, _):
         cols = pl.ds(pl.multiple_of(n * LANES, LANES), LANES)
@@ -907,18 +933,21 @@
         cols = slice(q * LANES, (q + 1) * LANES)
         kout[:, cols] = acc[q] * factor
 
-    arrived(fbuf, ids["fin"])
-    gw[:, ohalf] = fbuf[...]
-    for r in waits:
-        r.wait_send()
-
-    @pl.when(s < S - 1)
-    def _():
-        front.wait_send()
-
-    @pl.when(s > 0)
-    def _():
-        back.wait_send()
+    with jax.named_scope("finwait"):
+        arrived(fbuf, ids["fin"])
+    with jax.named_scope("fincopy"):
+        gw[:, ohalf] = fbuf[...]
+    with jax.named_scope("endwaits"):
+        for r in waits:
+            r.wait_send()
+
+        @pl.when(s < S - 1)
+        def _():
+            front.wait_send()
+
+        @pl.when(s > 0)
+        def _():
+            back.wait_send()
 
 
 def number(*sizes):
@@ -946,7 +975,7 @@
     M, CR = chunks // X, C // N
     ids, count = number(
         ("taps", S), ("front", 1), ("back", 1), ("w", 1), ("cot", X * 4), ("cotp", X * 2),
-        ("act", X * Z * Y), ("actp", X * Z * Y), ("ga", X * BLOCKS), ("y", (Y - 1) * Z * 2), ("zmid", Z), ("znear", 2), ("zfar", 2),
+        ("act", X * Z * Y), ("actp", X * Z * Y), ("ga", X * BLOCKS), ("y", (Y - 1) * Z * 3), ("zmid", Z // 2 * 3), ("znear", 3), ("zfar", 3),
         ("fin", 1),
         ("kg", S), ("k2", N),
     )

time: 69.4 us -> 66.6 us (0.960)
  Pallas kernels: 68.6 us -> 65.8 us
    pallas_call x1, Pallas kernels: 66.4 us -> 63.6 us  [pair_call(): pl.pallas_call(functools.partial(pair_kernel, S, N, Y, T, C, K, HB, ids),...]
where the time goes in v5:
time: 66.6 us; the launch traced here: 66.4 us
  Pallas kernels  65.8 us (99%)
    pallas_call x1, Pallas kernels, pair_call(): pl.pallas_call(functools.partial(pair_kernel, S, N, Y, T, C, K, HB, ids),...  63.6 us
    pallas_call x1, Pallas kernels, pair_call(): pl.pallas_call(functools.partial(hand_over, K), out_shape=(jax.ShapeDtype...  2.13 us

profile of v5, /device:TPU:0, one launch (start us, length us, event | category | flops | bytes accessed | tf_op | source)
XLA Modules:
  0.0 66.4 jit_solution(2470812301559897829)
XLA Ops:
  0.6 63.6 %block_backward.1 = (bf16[256,2048]{1,0:T(8,128)(2,1)S(1)}, bf16[256,2048]{1,0:T(8,128)(2,1)S(1)}, f32[64,2048]{1,0:T(8,128)S(1)}, f32[32,256]{1,0:T(8,128)S(1)}) custom-call(bf16[256,2048]{1,0:T(8,128)(2,1)} %bitcast.6, bf16[256,2048]{1,0:T(8,128)(2,1)} %bitcast.7, bf16[256,2048]{1,0:T(8,128)(2,1)} %bitcast.8, bf16[512,2048]{1,0:T(8,128)(2,1)} %w_in.1, ...), custom_call_target="tpu_custom_call" | custom-call | tf_op jit(solution)/shard_map/block_backward/pallas_call | solution.py:984
  64.3 2.1 %hand_over.1 = (bf16[256,2048]{1,0:T(8,128)(2,1)}, bf16[256,2048]{1,0:T(8,128)(2,1)}, f32[64,2048]{1,0:T(8,128)}, f32[31,256]{1,0:T(8,128)}, f32[1,256]{1,0:T(1,128)}) custom-call(bf16[256,2048]{1,0:T(8,128)(2,1)S(1)} %get-tuple-element.14.gv_in, bf16[256,2048]{1,0:T(8,128)(2,1)S(1)} %get-tuple-element.15.gg_in, f32[64,2048]{1,0:T(8,128)S(1)} %get-tuple-element.16.gw_in, ...), custom_call_target="tpu_custom_call" | custom-call | tf_op jit(solution)/shard_map/hand_over/pallas_call | solution.py:1047

commit v6 on v5

--- a/solution.py
+++ b/solution.py
@@ -315,7 +315,7 @@
 def pair_kernel(
     S, N, Y, T, C, K, HB, ids,
     cot_in, val_in, gate_in, w_in, kernel_in, gain_in,
-    gv, gg, gw, kout,
+    gv, gg, gw, kout, gout,
     kernel, gain, taps, cot, val, gate, w, w_p, cot_m, cot_p, fsend, frecv, bsend, brecv, ext, cen, gc, gext, kall,
     act, act_m, act_p, ga_s, ga, wacc, wpart, yrecv, ysum, zmid, zrecv, fin, fbuf,
     means, invs, sum1, sum2, kacc, kg, kgb, krecv, ksum, k2recv, send_sem, recv_sem, load_sem, ready,
@@ -409,7 +409,7 @@
             for side in range(2):
                 send(
                     cot.at[:, strip(side, p)], cot_m.at[j - 1, :, strip(side, p)],
-                    ids["cot"] + (j * 2 + p) * 2 + side, s, lax.rem(d + 2 * j, N),
+                    ids["cot"] + ((j - 1) * 2 + p) * 2 + side, s, lax.rem(d + 2 * j, N),
                 )
 
     send_cot(0)
@@ -451,7 +451,9 @@
             signal(ready.at[2 * (Z - 2)], z * Y + lax.rem(y + j, Y), d)
         pl.semaphore_wait(ready.at[2 * (Z - 2)], Y - 1)
     for j in range(1, S):
-        send(taps, kall.at[pl.ds(s * cps, cps)], ids["taps"] + j, lax.rem(s + j, S), d)
+        copy(taps, kall.at[pl.ds(s * cps, cps)], ids["taps"], lax.rem(s + j, S), d).start()
+    all_taps = kall.at[pl.ds(0, chunks - cps)]
+    waits.append(copy(all_taps, all_taps, ids["taps"], s, partner))
     front = copy(fsend, frecv, ids["front"], lax.rem(s + 1, S), d)
 
     @pl.when(s < S - 1)
@@ -474,8 +476,7 @@
     with jax.named_scope("proj_own"):
         project(cot, w, ga, d * cpd)
     with jax.named_scope("tapswait"):
-        for j in range(1, S):
-            arrived(kall.at[pl.ds(lax.rem(s + S - j, S) * cps, cps)], ids["taps"] + j)
+        arrived(all_taps, ids["taps"])
 
         @pl.when(s > 0)
         def _():
@@ -552,17 +553,17 @@
             for j in range(1, X):
                 send(
                     act.at[lax.rem(x + j, X), piece], act_m.at[j - 1, piece],
-                    ids["act"] + (j * Z + k) * Y + n, s, lax.rem(d + 2 * j, N),
+                    ids["act"] + (j - 1) * (Z - 1 + Y) + k + n, s, lax.rem(d + 2 * j, N),
                 )
 
     def relay_mirror(p):
         with jax.named_scope("cotwait%d" % p):
             for j in range(1, X):
                 for side in range(2):
-                    arrived(cot_m.at[j - 1, :, strip(side, p)], ids["cot"] + (j * 2 + p) * 2 + side)
+                    arrived(cot_m.at[j - 1, :, strip(side, p)], ids["cot"] + ((j - 1) * 2 + p) * 2 + side)
                 send(
                     cot_m.at[j - 1, :, strip(other, p)], cot_p.at[j, :, strip(0, p)],
-                    ids["cotp"] + j * 2 + p, s, partner,
+                    ids["cotm"] + (j - 1) * 2 + p, s, partner,
                 )
 
     def project_mirror():
@@ -574,7 +575,7 @@
                 rows = pl.ds(b * TB, TB)
                 send(
                     ga_s.at[j - 1, :, rows], ga.at[pl.ds(x * 2 * cpd, 2 * cpd), rows],
-                    ids["ga"] + j * BLOCKS + b, s, lax.rem(d + 2 * (X - j), N),
+                    ids["ga"] + (j - 1) * BLOCKS + b, s, lax.rem(d + 2 * (X - j), N),
                 )
 
     dims = (((1,), (0,)), ((), ()))
@@ -613,15 +614,15 @@
             for first, size, n in planes(k, own):
                 piece = pl.ds(first, size)
                 for j in range(1, X):
-                    i = (j * Z + k) * Y + n
+                    i = (j - 1) * (Z - 1 + Y) + k + n
                     arrived(act_m.at[j - 1, piece], ids["act"] + i)
-                    send(act_m.at[j - 1, piece], act_p.at[j, piece], ids["actp"] + i, s, partner)
+                    send(act_m.at[j - 1, piece], act_p.at[j, piece], ids["actm"] + i, s, partner)
 
     def relayed(k, own=False):
         with jax.named_scope("relaywait%d" % k):
             for first, size, n in planes(k, own):
                 for j in range(1, X):
-                    arrived(act_p.at[j, pl.ds(first, size)], ids["actp"] + (j * Z + k) * Y + n)
+                    arrived(act_p.at[j, pl.ds(first, size)], ids["actm"] + (j - 1) * (Z - 1 + Y) + k + n)
 
     def own_part(k, off, size):
         def own_tile(n, _):
@@ -639,7 +640,7 @@
         if k == 0 and p != 1:
             q = 0 if p == 0 else 1
             for j in range(1, X):
-                arrived(cot_p.at[j, :, strip(0, q)], ids["cotp"] + j * 2 + q)
+                arrived(cot_p.at[j, :, strip(0, q)], ids["cotm"] + (j - 1) * 2 + q)
         with jax.named_scope("wremote%d%d" % (k, p)):
             for j in range(1, Y):
                 to_y = lax.rem(y + j, Y)
@@ -728,7 +729,7 @@
         with jax.named_scope("gawait%d" % b):
             for j in range(1, X):
                 origin = lax.rem(x + j, X)
-                arrived(ga.at[pl.ds(origin * 2 * cpd, 2 * cpd), rows], ids["ga"] + j * BLOCKS + b)
+                arrived(ga.at[pl.ds(origin * 2 * cpd, 2 * cpd), rows], ids["ga"] + (X - j - 1) * BLOCKS + b)
 
         def grad_chunk(cb, sums):
             one, two = sums
@@ -761,7 +762,7 @@
 
     def kg_copy(off):
         to = lax.rem(s + off, S)
-        return copy(kgb.at[pl.ds(to * cps, cps)], krecv.at[off], ids["kg"] + off, to, d)
+        return copy(kgb.at[pl.ds(to * cps, cps)], krecv.at[off], ids["kg"], to, d)
 
     def taps_grad(b):
         def taps_chunk(cb, _):
@@ -869,7 +870,8 @@
     reduce_y(2, 1)
     gradient(3)
     taps_grad(3)
-    waits.extend(kg_copy(j) for j in range(1, S))
+    all_sums = krecv.at[pl.ds(1, S - 1)]
+    waits.append(copy(all_sums, all_sums, ids["kg"], s, partner))
     reduce_y(2, 2)
     relay_act(3, own=True)
     gated_grad(0)
@@ -884,14 +886,15 @@
         waits.clear()
         outer.clear()
     with jax.named_scope("kgwait"):
-        for j in range(1, S):
-            arrived(krecv.at[j], ids["kg"] + j)
+        arrived(all_sums, ids["kg"])
     acc = kg[pl.ds(s * cps, cps)]
     for j in range(1, S):
         acc = acc + krecv[j].astype(f32)
     ksum[...] = acc
     for j in range(1, N):
-        send(ksum, k2recv.at[j], ids["k2"] + j, s, lax.rem(d + j, N))
+        copy(ksum, k2recv.at[j], ids["k2"], s, lax.rem(d + j, N)).start()
+    all_parts = k2recv.at[pl.ds(1, N - 1)]
+    waits.append(copy(all_parts, all_parts, ids["k2"], s, partner))
     with jax.named_scope("zwait"):
         for p in range(P):
             arrived(zrecv.at[0, :, part(p)], ids["znear"] + p)
@@ -926,12 +929,13 @@
 
     gated_grad(3)
     with jax.named_scope("k2wait"):
+        arrived(all_parts, ids["k2"])
         for j in range(1, N):
-            arrived(k2recv.at[j], ids["k2"] + j)
             acc = acc + k2recv[j]
     for q in range(cps):
         cols = slice(q * LANES, (q + 1) * LANES)
-        kout[:, cols] = acc[q] * factor
+        kout[:, cols] = (acc[q] * factor)[:K]
+        gout[:, cols] = (acc[q] * factor)[K : K + 1]
 
     with jax.named_scope("finwait"):
         arrived(fbuf, ids["fin"])
@@ -958,13 +962,11 @@
     return ids, count
 
 
-def hand_over(K, gv_in, gg_in, gw_in, k_in, gv, gg, gw, kout, gout, sem):
-    pieces = ((gv_in, gv), (gg_in, gg), (gw_in, gw))
-    stores = [pltpu.make_async_copy(a, b, sem.at[i]) for i, (a, b) in enumerate(pieces)]
+def hand_over(*refs):
+    half = len(refs) // 2
+    stores = [pltpu.make_async_copy(refs[i], refs[half + i], refs[-1].at[i]) for i in range(half)]
     for st in stores:
         st.start()
-    kout[...] = k_in[:K]
-    gout[...] = k_in[K : K + 1]
     for st in stores:
         st.wait()
 
@@ -974,10 +976,10 @@
     chunks, cps, cpd, block = C // LANES, C // LANES // S, C // LANES // N, C // (S * N)
     M, CR = chunks // X, C // N
     ids, count = number(
-        ("taps", S), ("front", 1), ("back", 1), ("w", 1), ("cot", X * 4), ("cotp", X * 2),
-        ("act", X * Z * Y), ("actp", X * Z * Y), ("ga", X * BLOCKS), ("y", (Y - 1) * Z * 3), ("zmid", Z // 2 * 3), ("znear", 3), ("zfar", 3),
-        ("fin", 1),
-        ("kg", S), ("k2", N),
+        ("taps", 1), ("front", 1), ("back", 1), ("w", 1), ("cot", (X - 1) * 4), ("cotp", 1),
+        ("cotm", (X - 1) * 2), ("act", (X - 1) * (Z - 1 + Y)), ("actp", 1),
+        ("actm", (X - 1) * (Z - 1 + Y)), ("ga", (X - 1) * BLOCKS), ("y", (Y - 1) * Z * 3),
+        ("zmid", Z // 2 * 3), ("znear", 3), ("zfar", 3), ("fin", 1), ("kg", 1), ("k2", 1),
     )
     vm = pl.BlockSpec(memory_space=pltpu.VMEM)
     hbm = pl.BlockSpec(memory_space=pl.ANY)
@@ -987,10 +989,11 @@
             jax.ShapeDtypeStruct((T, C), bf16),
             jax.ShapeDtypeStruct((T, C), bf16),
             jax.ShapeDtypeStruct((block, C), f32),
-            jax.ShapeDtypeStruct((KP, C // S), f32),
+            jax.ShapeDtypeStruct((K, C // S), f32),
+            jax.ShapeDtypeStruct((1, C // S), f32),
         ),
         in_specs=[hbm] * 6,
-        out_specs=(vm,) * 4,
+        out_specs=(vm,) * 5,
         scratch_shapes=[
             pltpu.VMEM((K, C // S), bf16),
             pltpu.VMEM((C // S,), bf16),
@@ -1045,7 +1048,7 @@
         name="block_backward",
     )(*(pltpu.with_memory_space_constraint(a, pltpu.HBM) for a in (cot, val, gate, w, kernel, gain)))
     return pl.pallas_call(
-        functools.partial(hand_over, K),
+        hand_over,
         out_shape=(
             jax.ShapeDtypeStruct((T, C), bf16),
             jax.ShapeDtypeStruct((T, C), bf16),
@@ -1053,10 +1056,10 @@
             jax.ShapeDtypeStruct((K, C // S), f32),
             jax.ShapeDtypeStruct((1, C // S), f32),
         ),
-        in_specs=[vm] * 4,
-        out_specs=(hbm, hbm, hbm, vm, vm),
+        in_specs=[vm] * 5,
+        out_specs=(hbm,) * 5,
         scratch_shapes=[
-            pltpu.SemaphoreType.DMA((3,)),
+            pltpu.SemaphoreType.DMA((5,)),
         ],
         compiler_params=pltpu.CompilerParams(vmem_limit_bytes=16 * T * LANES),
         name="hand_over",

time: 66.6 us -> 65.1 us (0.977)
  Pallas kernels: 65.8 us -> 64.3 us
    pallas_call x1, Pallas kernels: 63.6 us -> 62.8 us  [pair_call(): pl.pallas_call(functools.partial(pair_kernel, S, N, Y, T, C, K, HB, ids),...]
where the time goes in v6:
time: 65.1 us; the launch traced here: 65 us
  Pallas kernels  64.3 us (99%)
    pallas_call x1, Pallas kernels, pair_call(): pl.pallas_call(functools.partial(pair_kernel, S, N, Y, T, C, K, HB, ids),...  62.8 us
    pallas_call x1, Pallas kernels, pair_call(): pl.pallas_call(hand_over, out_shape=(jax.ShapeDtypeStruct((T, C), bf16),...  1.53 us

profile of v6, /device:TPU:0, one launch (start us, length us, event | category | flops | bytes accessed | tf_op | source)
XLA Modules:
  0.0 65.0 jit_solution(14923216107420205725)
XLA Ops:
  0.6 62.8 %block_backward.1 = (bf16[256,2048]{1,0:T(8,128)(2,1)S(1)}, bf16[256,2048]{1,0:T(8,128)(2,1)S(1)}, f32[64,2048]{1,0:T(8,128)S(1)}, f32[31,256]{1,0:T(8,128)S(1)}, f32[1,256]{1,0:T(1,128)S(1)}) custom-call(bf16[256,2048]{1,0:T(8,128)(2,1)} %bitcast.6, bf16[256,2048]{1,0:T(8,128)(2,1)} %bitcast.7, bf16[256,2048]{1,0:T(8,128)(2,1)} %bitcast.8, ...), custom_call_target="tpu_custom_call" | custom-call | tf_op jit(solution)/shard_map/block_backward/pallas_call | solution.py:986
  63.4 1.5 %hand_over.1 = (bf16[256,2048]{1,0:T(8,128)(2,1)}, bf16[256,2048]{1,0:T(8,128)(2,1)}, f32[64,2048]{1,0:T(8,128)}, f32[31,256]{1,0:T(8,128)}, f32[1,256]{1,0:T(1,128)}) custom-call(bf16[256,2048]{1,0:T(8,128)(2,1)S(1)} %get-tuple-element.15.refs_0_, bf16[256,2048]{1,0:T(8,128)(2,1)S(1)} %get-tuple-element.16.refs_1_, ...), custom_call_target="tpu_custom_call" | custom-call | tf_op jit(solution)/shard_map/hand_over/pallas_call | solution.py:1050

commit v7 on v6

--- a/solution.py
+++ b/solution.py
@@ -318,7 +318,7 @@
     gv, gg, gw, kout, gout,
     kernel, gain, taps, cot, val, gate, w, w_p, cot_m, cot_p, fsend, frecv, bsend, brecv, ext, cen, gc, gext, kall,
     act, act_m, act_p, ga_s, ga, wacc, wpart, yrecv, ysum, zmid, zrecv, fin, fbuf,
-    means, invs, sum1, sum2, kacc, kg, kgb, krecv, ksum, k2recv, send_sem, recv_sem, load_sem, ready,
+    sigs, slopes, means, invs, sum1, sum2, kacc, kg, kgb, krecv, ksum, k2recv, send_sem, recv_sem, load_sem, ready,
 ):
     s = lax.axis_index("sp")
     d = lax.axis_index("dp")
@@ -337,9 +337,12 @@
     factor = float(S * N * T) ** (-0.5)
     waits = []
 
+    kinds = sorted(ids.values())
+
     def copy(src, dst, i, to_s, to_d, j=None):
+        kind = max(n for n, first in enumerate(kinds) if first <= i)
         return pltpu.make_async_remote_copy(
-            src_ref=src, dst_ref=dst, send_sem=send_sem.at[i],
+            src_ref=src, dst_ref=dst, send_sem=send_sem.at[kind],
             recv_sem=recv_sem.at[i if j is None else j],
             device_id={"sp": to_s, "dp": to_d}, device_id_type=pl.DeviceIdType.MESH,
         )
@@ -347,7 +350,8 @@
     def send(src, dst, i, to_s, to_d, j=None):
         r = copy(src, dst, i, to_s, to_d, j)
         r.start()
-        waits.append(r)
+        if i in (ids["w"], ids["cotp"], ids["actp"], ids["fin"]):
+            waits.append(r)
 
     def arrived(dst, i):
         copy(dst, dst, i, s, partner).wait_recv()
@@ -473,6 +477,15 @@
 
         lax.fori_loop(0, cpd // 2, pair, 0)
 
+    def slope_chunk(cb, _):
+        cols = pl.ds(pl.multiple_of(cb * LANES, LANES), LANES)
+        sig = jax.nn.sigmoid(gate[:, cols].astype(f32))
+        sigs[cb] = sig
+        slopes[cb] = val[:, cols].astype(f32) * sig * (1.0 - sig)
+        return _
+
+    with jax.named_scope("slopes"):
+        lax.fori_loop(0, chunks, slope_chunk, 0)
     with jax.named_scope("proj_own"):
         project(cot, w, ga, d * cpd)
     with jax.named_scope("tapswait"):
@@ -543,9 +556,11 @@
         return jnp.where(low, 0, near) + lax.rem(z + 1 + k, near)
 
     def planes(k, own):
-        if k < Z - 1:
-            return [(plane(k) * Y, Y, 0)]
-        return [(plane(k) * Y + lax.rem(y + j, Y), 1, j) for j in (range(1) if own else range(1, Y))]
+        first = k if k == 0 else k + Y - 1
+        if 0 < k < Z - 1:
+            return [(plane(k) * Y, Y, first)]
+        chosen = range(1) if own else range(1, Y)
+        return [(plane(k) * Y + lax.rem(y + j, Y), 1, first + j) for j in chosen]
 
     def send_act(k, own=False):
         for first, size, n in planes(k, own):
@@ -553,7 +568,7 @@
             for j in range(1, X):
                 send(
                     act.at[lax.rem(x + j, X), piece], act_m.at[j - 1, piece],
-                    ids["act"] + (j - 1) * (Z - 1 + Y) + k + n, s, lax.rem(d + 2 * j, N),
+                    ids["act"] + (j - 1) * (Z - 2 + 2 * Y) + n, s, lax.rem(d + 2 * j, N),
                 )
 
     def relay_mirror(p):
@@ -614,7 +629,7 @@
             for first, size, n in planes(k, own):
                 piece = pl.ds(first, size)
                 for j in range(1, X):
-                    i = (j - 1) * (Z - 1 + Y) + k + n
+                    i = (j - 1) * (Z - 2 + 2 * Y) + n
                     arrived(act_m.at[j - 1, piece], ids["act"] + i)
                     send(act_m.at[j - 1, piece], act_p.at[j, piece], ids["actm"] + i, s, partner)
 
@@ -622,7 +637,7 @@
         with jax.named_scope("relaywait%d" % k):
             for first, size, n in planes(k, own):
                 for j in range(1, X):
-                    arrived(act_p.at[j, pl.ds(first, size)], ids["actm"] + (j - 1) * (Z - 1 + Y) + k + n)
+                    arrived(act_p.at[j, pl.ds(first, size)], ids["actm"] + (j - 1) * (Z - 2 + 2 * Y) + n)
 
     def own_part(k, off, size):
         def own_tile(n, _):
@@ -657,7 +672,7 @@
                     ids["y"] + i * P + p, z * Y + to_y, d,
                 )
 
-            if k < Z - 1:
+            if 0 < k < Z - 1:
                 own_part(k, off, size)
 
     def reduce_y(k, p):
@@ -692,7 +707,6 @@
             def _():
                 r.start()
 
-            outer.append(r)
         elif k < Z - 1:
             send(
                 ysum.at[k, :, part(p)], zrecv.at[0, :, part(p)], ids["znear"] + p,
@@ -718,8 +732,6 @@
                 ysum.at[k, :, part(p)], zrecv.at[1, :, part(p)], ids["zmid"] + k * P + p,
                 to_z * Y + y, d, ids["zfar"] + p,
             ).start()
-
-    outer = []
 
     def fold(v):
         return jnp.sum(v.reshape(v.shape[0] // 8, 8, LANES), axis=0)
@@ -781,7 +793,7 @@
             return _
 
         def taps_owner(n, _):
-            off = 1 + lax.rem(n + S // 2 - 1, S - 1)
+            off = jnp.where(low, S - 1 - n, 1 + n)
             to = lax.rem(s + off, S)
             lax.fori_loop(to * cps, to * cps + cps, taps_chunk, 0)
             kg_copy(off).start()
@@ -804,9 +816,8 @@
             for k in range(K):
                 acc = acc + tf[k : k + 1] * gext[cb, pl.ds(k + b * TB, TB), :]
             acc = acc.astype(bf16).astype(f32)
-            sig = jax.nn.sigmoid(gate[rows, cols].astype(f32))
-            gv[rows, cols] = (acc * sig).astype(bf16)
-            gg[rows, cols] = (acc * val[rows, cols].astype(f32) * sig * (1.0 - sig)).astype(bf16)
+            gv[rows, cols] = (acc * sigs[cb, rows, :]).astype(bf16)
+            gg[rows, cols] = (acc * slopes[cb, rows, :]).astype(bf16)
             return _
 
         with jax.named_scope("gated%d" % b):
@@ -814,6 +825,7 @@
 
     back = copy(bsend, brecv, ids["back"], lax.rem(s + S - 1, S), d)
     send_act(0)
+    send_act(0, own=True)
     send_act(1)
     send_cot(1)
     send_act(2)
@@ -823,13 +835,16 @@
         project(cot, w_p, ga, partner * cpd)
     local_plane(0)
     local_plane(1)
-    local_plane(2)
     relay_mirror(0)
     relay_act(0)
+    local_plane(2)
     weight_part(0, 0)
     weight_part(0, 1)
+    relay_act(0, own=True)
+    local_plane(3)
     relay_act(1)
-    local_plane(3)
+    relayed(0, own=True)
+    own_part(0, 0, H - H // BLOCKS)
     weight_part(1, 0)
     weight_part(1, 1)
     relay_mirror(1)
@@ -838,6 +853,7 @@
     send_act(3, own=True)
     reduce_y(0, 1)
     weight_part(0, 2)
+    own_part(0, H - H // BLOCKS, H // BLOCKS)
     weight_part(1, 2)
     relay_act(2)
     reduce_y(1, 0)
@@ -881,16 +897,22 @@
     reduce_y(3, 0)
     gated_grad(2)
     with jax.named_scope("drain"):
-        for r in waits + outer:
+        for name, whole in (
+            ("cot", cot_m), ("cotm", cot_p.at[pl.ds(1, X - 1)]), ("act", act_m),
+            ("actm", act_p.at[pl.ds(1, X - 1)]), ("ga", ga_s), ("y", wpart), ("zmid", zmid),
+            ("znear", zrecv.at[0]),
+        ):
+            waits.append(copy(whole, whole, ids[name], s, partner))
+        for r in waits:
             r.wait_send()
         waits.clear()
-        outer.clear()
     with jax.named_scope("kgwait"):
         arrived(all_sums, ids["kg"])
     acc = kg[pl.ds(s * cps, cps)]
     for j in range(1, S):
         acc = acc + krecv[j].astype(f32)
-    ksum[...] = acc
+    ksum[...] = acc.astype(bf16)
+    acc = ksum[...].astype(f32)
     for j in range(1, N):
         copy(ksum, k2recv.at[j], ids["k2"], s, lax.rem(d + j, N)).start()
     all_parts = k2recv.at[pl.ds(1, N - 1)]
@@ -931,7 +953,7 @@
     with jax.named_scope("k2wait"):
         arrived(all_parts, ids["k2"])
         for j in range(1, N):
-            acc = acc + k2recv[j]
+            acc = acc + k2recv[j].astype(f32)
     for q in range(cps):
         cols = slice(q * LANES, (q + 1) * LANES)
         kout[:, cols] = (acc[q] * factor)[:K]
@@ -977,8 +999,8 @@
     M, CR = chunks // X, C // N
     ids, count = number(
         ("taps", 1), ("front", 1), ("back", 1), ("w", 1), ("cot", (X - 1) * 4), ("cotp", 1),
-        ("cotm", (X - 1) * 2), ("act", (X - 1) * (Z - 1 + Y)), ("actp", 1),
-        ("actm", (X - 1) * (Z - 1 + Y)), ("ga", (X - 1) * BLOCKS), ("y", (Y - 1) * Z * 3),
+        ("cotm", (X - 1) * 2), ("act", (X - 1) * (Z - 2 + 2 * Y)), ("actp", 1),
+        ("actm", (X - 1) * (Z - 2 + 2 * Y)), ("ga", (X - 1) * BLOCKS), ("y", (Y - 1) * Z * 3),
         ("zmid", Z // 2 * 3), ("znear", 3), ("zfar", 3), ("fin", 1), ("kg", 1), ("k2", 1),
     )
     vm = pl.BlockSpec(memory_space=pltpu.VMEM)
@@ -1027,6 +1049,8 @@
             pltpu.VMEM((2, LANES, H), bf16),
             pltpu.VMEM((2, block, H), f32),
             pltpu.VMEM((block, H), f32),
+            pltpu.VMEM((chunks, T, LANES), f32),
+            pltpu.VMEM((chunks, T, LANES), f32),
             pltpu.VMEM((T, LANES), f32),
             pltpu.VMEM((T, LANES), f32),
             pltpu.VMEM((T, LANES), f32),
@@ -1035,9 +1059,9 @@
             pltpu.VMEM((chunks, KP, LANES), f32),
             pltpu.VMEM((chunks, KP, LANES), bf16),
             pltpu.VMEM((S, cps, KP, LANES), bf16),
-            pltpu.VMEM((cps, KP, LANES), f32),
-            pltpu.VMEM((N, cps, KP, LANES), f32),
-            pltpu.SemaphoreType.DMA((count,)),
+            pltpu.VMEM((cps, KP, LANES), bf16),
+            pltpu.VMEM((N, cps, KP, LANES), bf16),
+            pltpu.SemaphoreType.DMA((len(ids),)),
             pltpu.SemaphoreType.DMA((count,)),
             pltpu.SemaphoreType.DMA((6,)),
             pltpu.SemaphoreType.REGULAR((2 * (Z - 2) + 1,)),

time: 65.1 us -> 64.5 us (level)
    pallas_call x1, Pallas kernels: 62.8 us -> 62.1 us  [pair_call(): pl.pallas_call(functools.partial(pair_kernel, S, N, Y, T, C, K, HB, ids),...]
where the time goes in v7:
time: 64.5 us; the launch traced here: 64.3 us
  Pallas kernels  63.7 us (99%)
    pallas_call x1, Pallas kernels, pair_call(): pl.pallas_call(functools.partial(pair_kernel, S, N, Y, T, C, K, HB, ids),...  62.1 us
    pallas_call x1, Pallas kernels, pair_call(): pl.pallas_call(hand_over, out_shape=(jax.ShapeDtypeStruct((T, C), bf16),...  1.53 us

profile of v7, /device:TPU:0, one launch (start us, length us, event | category | flops | bytes accessed | tf_op | source)
XLA Modules:
  0.0 64.3 jit_solution(4392884279440010816)
XLA Ops:
  0.6 62.1 %block_backward.1 = (bf16[256,2048]{1,0:T(8,128)(2,1)S(1)}, bf16[256,2048]{1,0:T(8,128)(2,1)S(1)}, f32[64,2048]{1,0:T(8,128)S(1)}, f32[31,256]{1,0:T(8,128)S(1)}, f32[1,256]{1,0:T(1,128)S(1)}) custom-call(bf16[256,2048]{1,0:T(8,128)(2,1)} %bitcast.6, bf16[256,2048]{1,0:T(8,128)(2,1)} %bitcast.7, bf16[256,2048]{1,0:T(8,128)(2,1)} %bitcast.8, ...), custom_call_target="tpu_custom_call" | custom-call | tf_op jit(solution)/shard_map/block_backward/pallas_call | solution.py:1008
  62.8 1.5 %hand_over.1 = (bf16[256,2048]{1,0:T(8,128)(2,1)}, bf16[256,2048]{1,0:T(8,128)(2,1)}, f32[64,2048]{1,0:T(8,128)}, f32[31,256]{1,0:T(8,128)}, f32[1,256]{1,0:T(1,128)}) custom-call(bf16[256,2048]{1,0:T(8,128)(2,1)S(1)} %get-tuple-element.15.refs_0_, bf16[256,2048]{1,0:T(8,128)(2,1)S(1)} %get-tuple-element.16.refs_1_, ...), custom_call_target="tpu_custom_call" | custom-call | tf_op jit(solution)/shard_map/hand_over/pallas_call | solution.py:1074
